TPU v7x, 32 devices: a whole 2x2x4 slice. The times are simulated.
32 devices in a mesh: gr: 2 (over x), sp: 8 (over z, y), tp: 2 (over core).
Axes of the slice: x: 2, y: 2, z: 4, core: 2. Of those that a mesh axis runs over, the one named last changes fastest.
Arguments:
- tokens: bfloat16 [8, 2048, 2048], P('gr', 'sp'), parts along dimension 0, may hold values from -6 to 6
- new_rows: bfloat16 [8, 2048], P('gr'), parts along dimension 0, may hold values from -6 to 6
- new_query: bfloat16 [8, 1024], P('gr', 'tp'), parts along dimension 0, may hold values from -6 to 6
- norm_gain: bfloat16 [2048], replicated, may hold values from 0.099609375 to 1.8984375
- key_weight: bfloat16 [2048, 1024], P('sp', 'tp'), may hold values from -0.125 to 0.125
- value_weight: bfloat16 [2048, 2048], P('sp', 'tp'), may hold values from -0.125 to 0.125
- input_weight: bfloat16 [2048, 16], replicated, may hold values from -0.125 to 0.125
- forget_weight: bfloat16 [2048, 16], replicated, may hold values from -0.125 to 0.125
- forget_bias: float32 [16], P('tp'), may hold values from 3 to 12
- gate_offsets: float32 [8, 2048, 2, 16], P('gr', 'sp', None, 'tp'), parts along dimension 0, may hold values from -6 to 250, as said below
Outputs:
- cache_keys: bfloat16 [16, 1024, 1024], P(('gr', 'sp'), None, 'tp'), parts along dimension 0
- cache_values: bfloat16 [16, 1024, 2048], P(('gr', 'sp'), None, 'tp'), parts along dimension 0
- cache_weights: float32 [16, 16, 1024], P(('gr', 'sp'), 'tp'), parts along dimension 0
- first_read: bfloat16 [8, 2048], P('gr', 'tp'), parts along dimension 0
There are 2 independent parts, one for each index of `gr`. A program takes and returns all parts, laid end to end along the dimension named above; an argument that names none is the same for every part. Nothing has to cross between parts.
Inputs may be any that keep to these rules, and one draw needn't show every extreme that they name: `gate_offsets`: entry 1 along the third dimension is never positive.
All inputs are finite; a program needn't handle non-finite values.
Results may differ from a plain program's by a relative error of at most 0.012.
The roundings to bfloat16 on the way count: a program that leaves them out, or rounds other values in their place, can miss the bound.
Values may be sent and summed in bfloat16 or wider, within the bound.
A program may use at most 64 MiB of HBM per device.

v0:
```python
import jax
import jax.numpy as jnp
from jax import lax
from jax.sharding import PartitionSpec as P

EPSILON = 1e-06


def prefix(x, axis, combine, identity):
    devices, index = (lax.axis_size(axis), lax.axis_index(axis))
    everything = lax.all_gather(x, axis)
    start = jnp.broadcast_to(jnp.asarray(identity, x.dtype), x.shape)

    def turn(k, before):
        at = devices - 1 - k
        reached = at > index
        new = combine(before, everything[at])
        return jnp.where(reached, new, before)

    return lax.fori_loop(0, devices, turn, start)


def normed_rows(source, norm_gain):
    widened = source.astype(jnp.float32)
    inverse_rms = lax.rsqrt(jnp.mean(widened * widened, axis=-1, keepdims=True) + EPSILON)
    return (widened * inverse_rms * norm_gain.astype(jnp.float32)).astype(jnp.bfloat16)


def suffix_sums(log_forget):
    flipped = jnp.cumsum(jnp.flip(log_forget, 1), axis=1)
    return jnp.flip(flipped, 1) - log_forget


def add_totals(earlier, following):
    return earlier + following


def partial_read(query_heads, key_heads, value_heads, log_weight, peak_log):
    scores = jnp.einsum("nhd,nshd->nsh", query_heads, key_heads, preferred_element_type=jnp.float32)
    weighted_terms = jnp.exp(log_weight - peak_log[:, None, :]) * scores
    rounded = weighted_terms.astype(jnp.bfloat16)
    numerator = jnp.einsum(
        "nsh,nshd->nhd", rounded, value_heads, preferred_element_type=jnp.float32
    )
    return (numerator, jnp.sum(weighted_terms, axis=1))


def finish_read(numerator, denominator, peak_log, query_heads, key_new, value_new, gate_new):
    peak_new = jnp.maximum(peak_log, gate_new)
    old_part = jnp.exp(peak_log - peak_new)
    own_score = jnp.einsum("nhd,nhd->nh", query_heads, key_new, preferred_element_type=jnp.float32)
    new_part = jnp.exp(gate_new - peak_new) * own_score
    total_value = old_part[..., None] * numerator + new_part[..., None] * value_new.astype(
        jnp.float32
    )
    total_weight = old_part * denominator + new_part
    return total_value / jnp.maximum(jnp.abs(total_weight), 1.0)[..., None]


def per_device(
    tokens,
    new_rows,
    new_query,
    norm_gain,
    key_weight,
    value_weight,
    input_weight,
    forget_weight,
    forget_bias,
    gate_offsets,
):
    seq_count, positions, model_width = tokens.shape
    heads_here = forget_bias.shape[0]
    key_size = key_weight.shape[1] // heads_here
    value_size = value_weight.shape[1] // heads_here
    group_size = lax.axis_size("sp")
    pieces = group_size // seq_count
    sub_rows = positions // pieces
    prompt_rows = seq_count * positions
    normed_all = jnp.concatenate(
        [
            normed_rows(tokens, norm_gain).reshape(prompt_rows, model_width),
            normed_rows(new_rows, norm_gain),
        ],
        axis=0,
    )
    key_sum = jnp.dot(
        normed_all,
        lax.all_gather(key_weight, "sp", axis=0, tiled=True),
        preferred_element_type=jnp.float32,
    )
    value_sum = jnp.dot(
        normed_all,
        lax.all_gather(value_weight, "sp", axis=0, tiled=True),
        preferred_element_type=jnp.float32,
    )
    keys_all = (key_sum * key_size ** (-0.5)).astype(jnp.bfloat16)
    values_all = value_sum.astype(jnp.bfloat16)
    head_start = lax.axis_index("tp") * heads_here
    input_all = lax.dynamic_slice_in_dim(
        jnp.dot(normed_all, input_weight, preferred_element_type=jnp.float32),
        head_start,
        heads_here,
        1,
    )
    forget_all = lax.dynamic_slice_in_dim(
        jnp.dot(normed_all, forget_weight, preferred_element_type=jnp.float32),
        head_start,
        heads_here,
        1,
    )
    key_rows = keys_all[:prompt_rows].reshape(seq_count, positions, heads_here * key_size)
    value_rows = values_all[:prompt_rows].reshape(seq_count, positions, heads_here * value_size)
    input_gate = (
        input_all[:prompt_rows].reshape(seq_count, positions, heads_here) + gate_offsets[:, :, 0, :]
    )
    log_forget = (
        jax.nn.log_sigmoid(
            forget_all[:prompt_rows].reshape(seq_count, positions, heads_here) + forget_bias
        )
        + gate_offsets[:, :, 1, :]
    )
    key_new = keys_all[prompt_rows:].reshape(seq_count, heads_here, key_size)
    value_new = values_all[prompt_rows:].reshape(seq_count, heads_here, value_size)
    gate_new = input_all[prompt_rows:]
    query_all = new_query.reshape(seq_count, heads_here, key_size)
    cache_keys, cache_values = (
        lax.all_to_all(
            key_rows.reshape(seq_count * pieces, sub_rows, heads_here * key_size),
            "sp",
            split_axis=0,
            concat_axis=1,
            tiled=True,
        ),
        lax.all_to_all(
            value_rows.reshape(seq_count * pieces, sub_rows, heads_here * value_size),
            "sp",
            split_axis=0,
            concat_axis=1,
            tiled=True,
        ),
    )
    totals = jnp.sum(log_forget, axis=1)
    tail_sum = prefix(totals, "sp", add_totals, jnp.zeros_like(totals))
    log_weight = input_gate + suffix_sums(log_forget) + tail_sum[:, None, :]
    peak_all = lax.pmax(jnp.max(log_weight, axis=1), "sp")
    numerator, denominator = partial_read(
        query_all,
        key_rows.reshape(seq_count, positions, heads_here, key_size),
        value_rows.reshape(seq_count, positions, heads_here, value_size),
        log_weight,
        peak_all,
    )
    numerator, denominator = lax.psum((numerator, denominator), "sp")
    cache_weight = lax.all_to_all(
        log_weight.reshape(seq_count * pieces, sub_rows, heads_here),
        "sp",
        split_axis=0,
        concat_axis=1,
        tiled=True,
    )
    read_out = finish_read(
        numerator, denominator, peak_all, query_all, key_new, value_new, gate_new
    )
    return (
        cache_keys,
        cache_values,
        jnp.transpose(cache_weight, (0, 2, 1)),
        read_out.reshape(seq_count, heads_here * value_size).astype(jnp.bfloat16),
    )


def solution(mesh):
    return jax.shard_map(
        per_device,
        mesh=mesh,
        in_specs=(
            P("gr", "sp", None),
            P("gr", None),
            P("gr", "tp"),
            P(),
            P("sp", "tp"),
            P("sp", "tp"),
            P(),
            P(),
            P("tp"),
            P("gr", "sp", None, "tp"),
        ),
        out_specs=(
            P(("gr", "sp"), None, "tp"),
            P(("gr", "sp"), None, "tp"),
            P(("gr", "sp"), "tp", None),
            P("gr", "tp"),
        ),
        check_vma=False,
    )
```

profile of v0, /device:TPU:0, one launch (start us, length us, event | category | flops | bytes accessed | tf_op | source)
XLA Modules:
  0.0 284.5 jit_solution(15401344887834810137)
XLA Ops:
  7.2 0.0 copy-start
  7.2 0.0 copy-start.6
  7.2 0.0 all-gather.5.cloned.1.call-start
  7.2 0.7 all-gather.5.cloned.1.call-update
  7.9 0.0 all-gather.7.cloned.1.call-start
  8.0 0.7 all-gather.7.cloned.1.call-update
  8.7 0.7 convert_element_type.38
  9.4 1.0 fusion.8
  10.4 3.3 %fusion = f32[4,256]{1,0:T(4,128)S(1)} fusion(bf16[4,256,2048]{2,1,0:T(8,128)(2,1)} %param.12), kind=kLoop, calls=%fused_computation.3 | loop fusion | flops 6290432 | bytes 4198400 | tf_op jit(solution)/shard_map/reduce_sum | solution.py:25
  13.8 0.1 fusion.10
  13.8 1.0 fusion.2
  14.9 0.0 copy-start.5
  14.9 0.0 copy-start.8
  14.9 0.0 copy-start.9
  14.9 1.3 fusion.27
  16.3 0.6 copy-done.2
  16.9 0.2 fusion.33
  17.0 0.2 rev.7
  17.2 2.3 reduce-window.6
  19.4 0.1 slice.46
  19.5 0.1 copy.30
  19.7 0.1 add_bitcast_fusion
  19.7 0.2 rev.8
  19.9 28.5 %all-gather.1 = f32[8,4,8]{2,1,0:T(4,128)S(1)} all-gather(f32[1,4,8]{2,1,0:T(4,128)S(1)} %bitcast.87), channel_id=2, replica_groups=mesh['gr'=2,'sp'=8,'tp'=2] {'sp'}, dimensions={0}, use_global_device_ids=true | all-gather | bytes 1152 | tf_op jit(solution)/shard_map/all_gather | solution.py:11
  48.4 3.4 %fusion.28 = f32[1028,16]{0,1:T(8,128)S(1)} fusion(bf16[2048,16]{0,1:T(8,128)(2,1)S(1)} %copy-done.9, bf16[4,2048]{1,0:T(4,128)(2,1)S(1)} %fusion.10, bf16[1024,2048]{1,0:T(8,128)(2,1)} %bitcast.77), kind=kOutput, calls=%fused_computation.53 | convolution fusion | flops 75792384 | bytes 4342016 | tf_op jit(solution)/shard_map/dot_general | solution.py:101
  51.8 0.4 while.16
  52.2 0.7 fusion.31
  52.9 3.7 %all-to-all-start.2 = ((f32[8,128,8]{1,2,0:T(8,128)}), f32[8,128,8]{1,2,0:T(8,128)S(1)}, u32[]{:S(2)}, u32[]{:S(2)}) async-start(f32[8,128,8]{1,2,0:T(8,128)} %bitcast.15), calls=%async_computation.2 | async-start | bytes 65536 | tf_op jit(solution)/shard_map/all_to_all | solution.py:155
  56.5 6.3 %all-gather.5.cloned.1.call-done = bf16[2048,512]{1,0:T(8,128)(2,1)} async-done(((bf16[256,512]{1,0:T(8,128)(2,1)}), bf16[2048,512]{1,0:T(8,128)(2,1)}) %all-gather.5.cloned.1.call-update) | async-done | bytes 2097168 | tf_op jit(solution)/shard_map/all_gather | solution.py:89
  62.8 5.2 %fusion.3 = bf16[1028,512]{1,0:T(8,128)(2,1)S(1)} fusion(bf16[2048,512]{1,0:T(8,128)(2,1)} %all-gather.5.cloned.1.call-done, bf16[4,2048]{1,0:T(4,128)(2,1)S(1)} %fusion.10, bf16[1024,2048]{1,0:T(8,128)(2,1)} %bitcast.78), kind=kOutput, calls=%fused_computation.9 | convolution fusion | flops 2165346304 | bytes 7360512 | tf_op jit(solution)/shard_map/dot_general | solution.py:87
  68.0 1.0 copy-done.4
  69.1 1.0 slice.44
  70.1 0.0 all-to-all-done.2
  70.1 3.6 %all-to-all-start = ((bf16[8,128,512]{2,1,0:T(8,128)(2,1)}), bf16[8,128,512]{2,1,0:T(8,128)(2,1)S(1)}, u32[]{:S(2)}, u32[]{:S(2)}) async-start(bf16[8,128,512]{2,1,0:T(8,128)(2,1)} %bitcast.1), calls=%async_computation | async-start | bytes 2097152 | tf_op jit(solution)/shard_map/all_to_all | solution.py:128
  73.7 82.1 %all-gather.7.cloned.1.call-done = bf16[2048,1024]{1,0:T(8,128)(2,1)} async-done(((bf16[256,1024]{1,0:T(8,128)(2,1)}), bf16[2048,1024]{1,0:T(8,128)(2,1)}) %all-gather.7.cloned.1.call-update) | async-done | bytes 4194320 | tf_op jit(solution)/shard_map/all_gather | solution.py:94
  155.8 8.0 %convolution_convert_fusion = bf16[1028,1024]{1,0:T(8,128)(2,1)S(1)} fusion(bf16[2048,1024]{1,0:T(8,128)(2,1)} %all-gather.7.cloned.1.call-done, bf16[4,2048]{1,0:T(4,128)(2,1)S(1)} %fusion.10, bf16[1024,2048]{1,0:T(8,128)(2,1)} %bitcast.79), kind=kOutput, calls=%fused_computation.7 | convolution fusion | flops 4321218560 | bytes 10510336 | tf_op jit(solution)/shard_map/dot_general | solution.py:92
  163.9 1.3 copy-done.3
  165.2 2.2 slice_bitcast_fusion
  167.4 0.0 all-to-all-done
  167.4 4.4 %all-to-all-start.1 = ((bf16[8,128,1024]{2,1,0:T(8,128)(2,1)}), bf16[8,128,1024]{2,1,0:T(8,128)(2,1)}, u32[]{:S(2)}, u32[]{:S(2)}) async-start(bf16[8,128,1024]{2,1,0:T(8,128)(2,1)} %bitcast.3), calls=%async_computation.1 | async-start | bytes 4194304 | tf_op jit(solution)/shard_map/all_to_all | solution.py:135
  171.8 0.1 reshape.80
  171.9 0.1 reshape.95
  172.0 0.1 copy.32
  172.0 48.1 %pmax.7 = f32[4,8]{0,1:T(8,128)S(1)} all-reduce(f32[4,8]{0,1:T(8,128)S(1)} %copy.32), channel_id=1, replica_groups=mesh['gr'=2,'sp'=8,'tp'=2] {'sp'}, use_global_device_ids=true, to_apply=%region_8.9 | all-reduce | flops 32 | bytes 256 | tf_op jit(solution)/shard_map/pmax | solution.py:146
  220.2 0.1 copy.34
  220.3 3.9 %reshape.93 = bf16[4,256,8,64]{3,2,1,0:T(8,128)(2,1)} reshape(bf16[1024,512]{1,0:T(8,128)(2,1)} %slice.44) | data formatting | bytes 2097152 | tf_op jit(solution)/shard_map/reshape;reshape | solution.py:149
  224.2 0.1 reshape.81
  224.2 0.1 fusion.19
  224.3 0.1 copy.48
  224.4 2.2 fusion.4
  226.6 0.9 convert_bitcast_fusion.1
  227.6 0.1 copy.37
  227.7 0.6 copy.53
  228.3 0.4 fusion.6
  228.7 42.6 %all-reduce = (f32[4,8]{0,1:T(8,128)S(1)}, f32[4,8,128]{2,1,0:T(8,128)S(1)}) all-reduce(f32[4,8]{0,1:T(8,128)S(1)} %copy.37, f32[4,8,128]{2,1,0:T(8,128)S(1)} %bitcast.86), channel_id=1, replica_groups=mesh['gr'=2,'sp'=8,'tp'=2] {'sp'}, use_global_device_ids=true, to_apply=%region_11.12 | all-reduce | flops 4128 | bytes 33024 | tf_op jit(solution)/shard_map/psum | solution.py:154
  271.3 0.1 copy.38
  271.4 0.1 copy.33
  271.5 0.1 copy.36
  271.5 0.7 convert_bitcast_fusion
  272.3 0.1 fusion.20
  272.4 0.6 copy.71
  273.0 1.0 copy.81
  273.9 3.1 %copy.82 = bf16[1,1024,1024]{2,1,0:T(8,128)(2,1)} copy(bf16[1,1024,1024]{2,1,0:T(8,128)(2,1)} %bitcast.4) | data formatting | bytes 4194304
  277.0 0.6 copy.83
  (32 shorter events, 0.2 us)
Async XLA Ops:
  7.2 7.7 %copy-start = (bf16[2048,16]{0,1:T(8,128)(2,1)S(1)}, bf16[2048,16]{0,1:T(8,128)(2,1)}, u32[]{:S(2)}) copy-start(bf16[2048,16]{0,1:T(8,128)(2,1)} %param.19) | copy-start | bytes 196612
  7.2 6.6 %copy-start.6 = (bf16[4,2048]{1,0:T(4,128)(2,1)S(1)}, bf16[4,2048]{1,0:T(4,128)(2,1)}, u32[]{:S(2)}) copy-start(bf16[4,2048]{1,0:T(4,128)(2,1)} %param.13) | copy-start | bytes 49156
  7.2 55.6 %all-gather.5.cloned.1.call-start = ((), (), s32[]{:S(2)}) async-start(), calls=%async_computation.3 | async-start | bytes 2359296 | tf_op jit(solution)/shard_map/all_gather | solution.py:89
  7.9 147.9 %all-gather.7.cloned.1.call-start = ((), (), s32[]{:S(2)}) async-start(), calls=%async_computation.4 | async-start | bytes 4718592 | tf_op jit(solution)/shard_map/all_gather | solution.py:94
  9.4 4.5 %copy-start.1 = (bf16[4,256,2048]{2,1,0:T(8,128)(2,1)S(1)}, bf16[4,256,2048]{2,1,0:T(8,128)(2,1)}, u32[]{:S(2)}) copy-start(bf16[4,256,2048]{2,1,0:T(8,128)(2,1)} %param.12) | copy-start | bytes 12582916
  14.9 2.0 copy-start.2
  14.9 1.9 copy-start.5
  14.9 1.9 copy-start.8
  14.9 33.4 %copy-start.9 = (bf16[2048,16]{0,1:T(8,128)(2,1)S(1)}, bf16[2048,16]{0,1:T(8,128)(2,1)}, u32[]{:S(2)}) copy-start(bf16[2048,16]{0,1:T(8,128)(2,1)} %param.18) | copy-start | bytes 196612
  52.9 17.3 %all-to-all-start.2 = ((f32[8,128,8]{1,2,0:T(8,128)}), f32[8,128,8]{1,2,0:T(8,128)S(1)}, u32[]{:S(2)}, u32[]{:S(2)}) async-start(f32[8,128,8]{1,2,0:T(8,128)} %bitcast.15), calls=%async_computation.2 | async-start | bytes 65536 | tf_op jit(solution)/shard_map/all_to_all | solution.py:155
  68.0 1.0 copy-start.4
  70.1 97.3 %all-to-all-start = ((bf16[8,128,512]{2,1,0:T(8,128)(2,1)}), bf16[8,128,512]{2,1,0:T(8,128)(2,1)S(1)}, u32[]{:S(2)}, u32[]{:S(2)}) async-start(bf16[8,128,512]{2,1,0:T(8,128)(2,1)} %bitcast.1), calls=%async_computation | async-start | bytes 2097152 | tf_op jit(solution)/shard_map/all_to_all | solution.py:128
  163.8 1.3 copy-start.3
  165.2 6.6 %copy-start.7 = (bf16[4,512]{1,0:T(4,128)(2,1)S(1)}, bf16[4,512]{1,0:T(4,128)(2,1)}, u32[]{:S(2)}) copy-start(bf16[4,512]{1,0:T(4,128)(2,1)} %param.14) | copy-start | bytes 12292
  167.4 56.8 %slice-start = ((bf16[1028,512]{1,0:T(8,128)(2,1)}), bf16[4,512]{1,0:T(4,128)(2,1)S(1)}, s32[]{:S(2)}) async-start(bf16[1028,512]{1,0:T(8,128)(2,1)} %copy-done.4), calls=%async_computation.5 | async-start | bytes 8192 | tf_op jit(solution)/shard_map/slice | solution.py:123
  167.4 105.6 %all-to-all-start.1 = ((bf16[8,128,1024]{2,1,0:T(8,128)(2,1)}), bf16[8,128,1024]{2,1,0:T(8,128)(2,1)}, u32[]{:S(2)}, u32[]{:S(2)}) async-start(bf16[8,128,1024]{2,1,0:T(8,128)(2,1)} %bitcast.3), calls=%async_computation.1 | async-start | bytes 4194304 | tf_op jit(solution)/shard_map/all_to_all | solution.py:135
Sparse Core Ops, SparseCore 0:
  10.1 52.6 all-gather.4
  64.9 90.8 all-gather.6
where the time goes:
time: 285 us; the launch traced here: 284 us
  blocking collectives  119 us (42%)
  waiting for transfers between devices  89.7 us (31%)
  matrix products  20.6 us (7%)
  local copies, waits for them, and re-layouts  17.4 us (6%)
  between operations  14.2 us (5%)
  starting transfers between devices  11.7 us (4%)
  other arithmetic  11.3 us (4%)
    all_gather x1, waiting for transfers between devices, per_device(): lax.all_gather(value_weight, 'sp', axis=0, tiled=True)  82.1 us
    pmax x1, blocking collectives, per_device(): peak_all = lax.pmax(jnp.max(log_weight, axis=1), 'sp')  48.1 us
    psum x1, blocking collectives, per_device(): numerator, denominator = lax.psum((numerator, denominator), 'sp')  42.6 us
    all_gather x1, blocking collectives, prefix(): everything = lax.all_gather(x, axis)  28.5 us
    unnamed x26, local copies, waits for them, and re-layouts  11.1 us
    dot_general x1, matrix products, per_device(): jnp.dot(normed_all, lax.all_gather(value_weight, 'sp', axis=0, tiled=True...  8.03 us
    all_gather x1, waiting for transfers between devices, per_device(): lax.all_gather(key_weight, 'sp', axis=0, tiled=True)  6.26 us
  transfers between devices with their start and end apart: 5, of which 2 were waited for; matrix products, arithmetic and copies ran while one was open for 15% of the time, Pallas kernels for 0%

commit v1 on v0

v1 whole, which is shorter than its diff:
```python
import jax
import jax.numpy as jnp
from jax import lax
from jax.sharding import PartitionSpec as P

EPSILON = 1e-06
HIGHEST = lax.Precision.HIGHEST


def normed_rows(source, norm_gain):
    widened = source.astype(jnp.float32)
    inverse_rms = lax.rsqrt(jnp.mean(widened * widened, axis=-1, keepdims=True) + EPSILON)
    return (widened * inverse_rms * norm_gain.astype(jnp.float32)).astype(jnp.bfloat16)


def contract_last(a, b):
    return lax.dot_general(a, b, (((1,), (1,)), ((), ())), preferred_element_type=jnp.float32)


def log_weights(gates, offsets, forget_bias, heads, blocks, pieces):
    rows = gates.shape[1]
    sub = rows // blocks
    input_gate = gates[:heads] + offsets[:heads]
    log_forget = jax.nn.log_sigmoid(gates[heads:] + forget_bias[:, None]) + offsets[heads:]
    by_block = log_forget.reshape(heads, blocks, sub)
    later = jnp.tril(jnp.ones((sub, sub), jnp.float32), -1)
    within = jnp.dot(by_block.reshape(heads * blocks, sub), later, precision=HIGHEST)
    totals = jnp.sum(by_block, axis=2)
    index = lax.axis_index("sp")
    everything = lax.all_gather(totals, "sp")
    ours = lax.dynamic_slice_in_dim(everything, index // pieces * pieces, pieces, 0)
    piece = index % pieces
    all_pieces = jnp.sum(ours, axis=0)
    after = jnp.flip(jnp.cumsum(jnp.flip(all_pieces, 1), axis=1), 1) - all_pieces
    follows = (jnp.arange(pieces) > piece).astype(jnp.float32)
    after = after + jnp.sum(ours * follows[:, None, None], axis=0)
    suffix = within.reshape(heads, blocks, sub) + after[:, :, None]
    return input_gate + suffix.reshape(heads, rows)


def read_part(query, keys, values, log_weight, heads):
    key_size = keys.shape[1] // heads
    value_size = values.shape[1] // heads
    peak = jnp.max(log_weight, axis=1, keepdims=True)
    own_head = jnp.arange(heads)[:, None] == jnp.arange(keys.shape[1])[None, :] // key_size
    spread = jnp.where(own_head, query, jnp.zeros_like(query))
    scores = contract_last(spread, keys)
    terms = jnp.exp(log_weight - peak) * scores
    wide = jnp.dot(terms.astype(jnp.bfloat16), values, preferred_element_type=jnp.float32)
    pick = jnp.eye(heads, dtype=jnp.float32)
    numerator = jnp.sum(wide.reshape(heads, heads, value_size) * pick[:, :, None], axis=1)
    return peak, numerator, jnp.sum(terms, axis=1, keepdims=True)


def finish(peak, numerator, denominator, own_score, gate_new, value_new, seq_count, pieces):
    heads, value_size = numerator.shape
    one = jnp.concatenate([peak, denominator, own_score, gate_new], axis=1)
    one = jnp.pad(one, ((0, 0), (0, value_size - one.shape[1])))
    packed = jnp.concatenate([numerator, value_new, one], axis=1)
    everything = lax.all_gather(packed, "sp").reshape(seq_count, pieces, heads, -1)
    one = everything[..., 2 * value_size :]
    peaks, denominators = one[..., 0], one[..., 1]
    own_score, gate_new = one[:, 0, :, 2], one[:, 0, :, 3]
    value_new = everything[:, 0, :, value_size : 2 * value_size]
    top = jnp.maximum(jnp.max(peaks, axis=1), gate_new)
    old = jnp.exp(peaks - top[:, None])
    new = jnp.exp(gate_new - top) * own_score
    total = jnp.sum(old[..., None] * everything[..., :value_size], axis=1)
    total = total + new[..., None] * value_new
    weight = jnp.sum(old * denominators, axis=1) + new
    return total / jnp.maximum(jnp.abs(weight), 1.0)[..., None]


def per_device(
    tokens,
    new_rows,
    new_query,
    norm_gain,
    key_weight,
    value_weight,
    input_weight,
    forget_weight,
    forget_bias,
    gate_offsets,
):
    seq_count, positions, model_width = tokens.shape
    heads = forget_bias.shape[0]
    key_size = key_weight.shape[1] // heads
    group = lax.axis_size("sp")
    shares = lax.axis_size("tp")
    pieces = group // seq_count
    sub = positions // pieces
    rows = group * sub
    index, core = lax.axis_index("sp"), lax.axis_index("tp")
    prompt = index // pieces

    part = model_width // shares
    mine = lax.dynamic_slice_in_dim(tokens.reshape(group, sub, model_width), core * part, part, 2)
    moved = lax.all_to_all(mine, "sp", split_axis=0, concat_axis=0, tiled=True)
    source = lax.all_gather(moved.reshape(rows, part), "tp", axis=1, tiled=True)
    offsets = jnp.transpose(gate_offsets.reshape(group, sub, 2 * heads), (0, 2, 1))
    offsets = lax.all_to_all(offsets, "sp", split_axis=0, concat_axis=0, tiled=True)
    offsets = jnp.transpose(offsets, (1, 0, 2)).reshape(2 * heads, rows)
    key_weight = lax.all_gather(key_weight, "sp", axis=0, tiled=True)
    value_weight = lax.all_gather(value_weight, "sp", axis=0, tiled=True)

    normed = normed_rows(source, norm_gain)
    fresh = normed_rows(lax.dynamic_slice_in_dim(new_rows, prompt, 1, 0), norm_gain)
    head_start = core * heads
    gate_weight = jnp.concatenate(
        [
            lax.dynamic_slice_in_dim(input_weight, head_start, heads, 1),
            lax.dynamic_slice_in_dim(forget_weight, head_start, heads, 1),
        ],
        axis=1,
    ).T
    gates = contract_last(gate_weight, normed)
    gate_new = contract_last(gate_weight[:heads], fresh)

    def project(x):
        keys = jnp.dot(x, key_weight, preferred_element_type=jnp.float32) * key_size**-0.5
        values = jnp.dot(x, value_weight, preferred_element_type=jnp.float32)
        return keys.astype(jnp.bfloat16), values.astype(jnp.bfloat16)

    keys, values = project(normed)
    key_new, value_new = project(fresh)
    log_weight = log_weights(gates, offsets, forget_bias, heads, group, pieces)
    query = lax.dynamic_slice_in_dim(new_query, prompt, 1, 0)
    peak, numerator, denominator = read_part(query, keys, values, log_weight, heads)
    own_score = jnp.sum(
        (query.astype(jnp.float32) * key_new.astype(jnp.float32)).reshape(heads, key_size),
        axis=1,
        keepdims=True,
    )
    value_new = value_new.astype(jnp.float32).reshape(heads, -1)
    read_out = finish(
        peak, numerator, denominator, own_score, gate_new, value_new, seq_count, pieces
    )
    return (
        keys[None],
        values[None],
        log_weight[None],
        read_out.reshape(seq_count, -1).astype(jnp.bfloat16),
    )


def solution(mesh):
    return jax.shard_map(
        per_device,
        mesh=mesh,
        in_specs=(
            P("gr", "sp", None),
            P("gr", None),
            P("gr", "tp"),
            P(),
            P("sp", "tp"),
            P("sp", "tp"),
            P(),
            P(),
            P("tp"),
            P("gr", "sp", None, "tp"),
        ),
        out_specs=(
            P(("gr", "sp"), None, "tp"),
            P(("gr", "sp"), None, "tp"),
            P(("gr", "sp"), "tp", None),
            P("gr", "tp"),
        ),
        check_vma=False,
    )
```

time: 285 us -> 264 us (0.926)
  blocking collectives: 119 us -> 142 us
  waiting for transfers between devices: 89.7 us -> 73.4 us
  local copies, waits for them, and re-layouts: 17.4 us -> 3.73 us
  starting transfers between devices: 11.7 us -> 3.71 us
  other arithmetic: 11.3 us -> 5.59 us
    all_to_all x0 -> x1, blocking collectives: none -> 80.9 us  [per_device(): moved = lax.all_to_all(mine, 'sp', split_axis=0, concat_axis=0, tiled=True)]
    pmax x1 -> x0, blocking collectives: 48.1 us -> none  [per_device(): peak_all = lax.pmax(jnp.max(log_weight, axis=1), 'sp')]
    psum x1 -> x0, blocking collectives: 42.6 us -> none  [per_device(): numerator, denominator = lax.psum((numerator, denominator), 'sp')]
    all_gather x1 -> x2, blocking collectives: 28.5 us -> 61.5 us  [the longest x1 30.9 us: log_weights(): everything = lax.all_gather(totals, 'sp')]
    all_gather x2 -> x3, waiting for transfers between devices: 88.4 us -> 72 us  [the longest x1 61.1 us: per_device(): value_weight = lax.all_gather(value_weight, 'sp', axis=0, tiled=True)]
    unnamed x26 -> x30, local copies, waits for them, and re-layouts: 11.1 us -> 0.6 us
    all_to_all x3 -> x1, starting transfers between devices: 11.6 us -> 3.59 us  [per_device(): lax.all_to_all(offsets, 'sp', split_axis=0, concat_axis=0, tiled=True)]
    another operation x3 -> x0, local copies, waits for them, and re-layouts: 3.9 us -> none  [the longest x1 3.89 us: per_device(): key_rows.reshape(seq_count, positions, heads_here, key_size)]
  transfers between devices with their start and end apart: 5 -> 4, of which waited for: 2 -> 2; matrix products, arithmetic and copies ran while one was open for 15% -> 5% of each run, Pallas kernels for 0% -> 0%
where the time goes in v1:
time: 264 us; the launch traced here: 263 us
  blocking collectives  142 us (54%)
  waiting for transfers between devices  73.4 us (28%)
  matrix products  19.9 us (8%)
  between operations  14.8 us (6%)
  other arithmetic  5.59 us (2%)
  local copies, waits for them, and re-layouts  3.73 us (1%)
  starting transfers between devices  3.71 us (1%)
    all_to_all x1, blocking collectives, per_device(): moved = lax.all_to_all(mine, 'sp', split_axis=0, concat_axis=0, tiled=True)  80.9 us
    all_gather x1, waiting for transfers between devices, per_device(): value_weight = lax.all_gather(value_weight, 'sp', axis=0, tiled=True)  61.1 us
    all_gather x1, blocking collectives, log_weights(): everything = lax.all_gather(totals, 'sp')  30.9 us
    all_gather x1, blocking collectives, finish(): lax.all_gather(packed, 'sp').reshape(seq_count, pieces, heads, -1)  30.5 us
    all_gather x1, waiting for transfers between devices, per_device(): source = lax.all_gather(moved.reshape(rows, part), 'tp', axis=1, tiled=True)  10.9 us
    dot_general x2, matrix products, project(): values = jnp.dot(x, value_weight, preferred_element_type=jnp.float32)  10.8 us
    dot_general x2, matrix products, project(): jnp.dot(x, key_weight, preferred_element_type=jnp.float32)  6.53 us
  transfers between devices with their start and end apart: 4, of which 2 were waited for; matrix products, arithmetic and copies ran while one was open for 5% of the time, Pallas kernels for 0%

profile of v1, /device:TPU:0, one launch (start us, length us, event | category | flops | bytes accessed | tf_op | source)
XLA Modules:
  0.0 263.4 jit_solution(13032726843708910737)
XLA Ops:
  7.2 0.0 all-gather.8.cloned.1.call-start
  7.2 0.7 all-gather.8.cloned.1.call-update
  7.9 0.0 all-gather.10.cloned.1.call-start
  7.9 0.7 all-gather.10.cloned.1.call-update
  8.6 0.0 all-gather.6.cloned.1.call-start
  8.7 1.8 constant_dynamic-slice_fusion.4
  10.5 0.0 copy-start.5
  10.5 0.0 copy-start.6
  10.5 0.0 copy-start.9
  10.5 0.0 copy-start.10
  10.5 0.0 copy-start.7
  10.5 0.0 copy-start.8
  10.5 80.9 %all_to_all.10 = bf16[8,128,1024]{2,1,0:T(8,128)(2,1)} all-to-all(bf16[8,128,1024]{2,1,0:T(8,128)(2,1)S(1)} %constant_dynamic-slice_fusion.4), channel_id=1, replica_groups=mesh['gr'=2,'sp'=8,'tp'=2] {'sp'}, dimensions={0} | all-to-all | bytes 4194304 | tf_op jit(solution)/shard_map/all_to_all | solution.py:99
  91.4 0.0 all-gather.6.cloned.1.call-update
  91.4 0.0 copy-done.5
  91.5 0.6 copy.36
  92.2 3.6 %all-to-all-start.1 = ((f32[8,16,128]{2,1,0:T(8,128)}), f32[8,16,128]{2,1,0:T(8,128)S(1)}, u32[]{:S(2)}, u32[]{:S(2)}) async-start(f32[8,16,128]{2,1,0:T(8,128)} %copy.36), calls=%async_computation.1 | async-start | bytes 131072 | tf_op jit(solution)/shard_map/all_to_all | solution.py:102
  95.8 0.0 copy-done.6
  95.8 0.6 multiply_reduce_fusion
  97.1 0.0 copy-done.9
  97.1 0.0 copy-done.10
  97.2 0.0 copy-done.7
  97.2 0.0 copy-done.8
  97.3 0.1 convolution_bitcast_fusion.1
  97.4 2.0 fusion.27
  99.4 0.1 reshape.181
  99.5 0.1 reduce_sum.99
  99.6 0.1 copy.43
  99.7 61.1 %all-gather.10.cloned.1.call-done = bf16[2048,1024]{1,0:T(8,128)(2,1)} async-done(((bf16[256,1024]{1,0:T(8,128)(2,1)}), bf16[2048,1024]{1,0:T(8,128)(2,1)}) %all-gather.10.cloned.1.call-update) | async-done | bytes 4194320 | tf_op jit(solution)/shard_map/all_gather | solution.py:105
  160.8 2.8 %fusion.29 = f32[1,1024]{1,0:T(1,128)S(1)} fusion(bf16[2048,1024]{1,0:T(8,128)(2,1)} %all-gather.10.cloned.1.call-done, bf16[1,2048]{1,0:T(2,128)(2,1)S(1)} %multiply_multiply_fusion), kind=kOutput, calls=%fused_computation.55 | convolution fusion | flops 4194304 | bytes 4202496 | tf_op jit(solution)/shard_map/dot_general | solution.py:122
  163.6 10.9 %all-gather.6.cloned.1.call-done = bf16[1024,2048]{1,0:T(8,128)(2,1)} async-done(((bf16[1024,1024]{1,0:T(8,128)(2,1)}), bf16[1024,2048]{1,0:T(8,128)(2,1)}) %all-gather.6.cloned.1.call-update) | async-done | bytes 4194320 | tf_op jit(solution)/shard_map/all_gather | solution.py:100
  174.6 3.2 %fusion = f32[1024]{0:T(1024)S(1)} fusion(bf16[1024,2048]{1,0:T(8,128)(2,1)} %all-gather.6.cloned.1.call-done), kind=kLoop, calls=%fused_computation.2 | loop fusion | flops 6290432 | bytes 4198400 | tf_op jit(solution)/shard_map/reduce_sum | solution.py:12
  177.8 0.0 copy-start.11
  177.8 0.2 copy-done
  178.0 1.3 fusion.9
  179.3 0.0 all-to-all-done.1
  179.3 0.0 copy-done.11
  179.3 0.2 fusion.52
  179.5 0.1 copy.38
  179.5 30.9 %all-gather = f32[64,8]{1,0:T(8,128)S(1)} all-gather(f32[8,8]{1,0:T(8,128)S(1)} %copy.38), channel_id=2, replica_groups=mesh['gr'=2,'sp'=8,'tp'=2] {'sp'}, dimensions={0}, use_global_device_ids=true | all-gather | bytes 2304 | tf_op jit(solution)/shard_map/all_gather | solution.py:30
  210.5 0.1 copy.46
  210.6 0.1 copy.45
  210.7 0.1 multiply_reduce_fusion.1
  210.8 0.1 copy.40
  210.9 0.3 fusion.4
  211.1 0.1 fusion.50
  211.3 0.1 copy.41
  211.3 0.0 copy-done.1
  211.3 4.6 %multiply_convert_fusion = bf16[1024,512]{1,0:T(8,128)(2,1)S(1)} fusion(bf16[2048,512]{1,0:T(8,128)(2,1)S(1)} %copy-done.1, bf16[1024,2048]{1,0:T(8,128)(2,1)} %all-gather.6.cloned.1.call-done, f32[2048]{0:T(1024)S(1)} %convert_element_type.64, f32[1024]{0:T(1024)S(1)} %add_rsqrt_fusion), kind=kOutput, calls=%fused_computation.5 | convolution fusion | flops 2156920832 | bytes 7352320 | tf_op jit(solution)/shard_map/dot_general | solution.py:121
  215.9 0.0 copy-start.3
  215.9 0.5 fusion.54
  216.4 0.1 copy.42
  216.5 8.0 %convolution_convert_fusion = bf16[1024,1024]{1,0:T(8,128)(2,1)S(1)} fusion(bf16[2048,1024]{1,0:T(8,128)(2,1)} %all-gather.10.cloned.1.call-done, bf16[1024,2048]{1,0:T(8,128)(2,1)} %all-gather.6.cloned.1.call-done, f32[2048]{0:T(1024)S(1)} %convert_element_type.64, f32[1024]{0:T(1024)S(1)} %add_rsqrt_fusion), kind=kOutput, calls=%fused_computation.6 | convolution fusion | flops 4304404480 | bytes 10498048 | tf_op jit(solution)/shard_map/dot_general | solution.py:122
  224.5 0.0 copy-start.2
  224.6 0.4 fusion.5
  224.9 0.1 select_maximum_fusion
  225.0 30.5 %all-gather.1 = f32[64,384]{1,0:T(8,128)S(1)} all-gather(f32[8,384]{1,0:T(8,128)S(1)} %pad_maximum_fusion.2), channel_id=3, replica_groups=mesh['gr'=2,'sp'=8,'tp'=2] {'sp'}, dimensions={0}, use_global_device_ids=true | all-gather | bytes 110592 | tf_op jit(solution)/shard_map/all_gather | solution.py:60
  255.6 0.1 slice_reduce_fusion.2
  255.7 0.2 slice_reduce_fusion.3
  255.8 0.2 exponential_reduce_fusion
  256.0 0.1 fusion.13
  256.2 0.1 broadcast_bitcast_fusion
  256.2 0.1 broadcast_bitcast_fusion.1
  256.3 0.6 fusion.24
  (32 shorter events, 0.3 us)
Async XLA Ops:
  7.2 90.2 %all-gather.8.cloned.1.call-start = ((), (), s32[]{:S(2)}) async-start(), calls=%async_computation.3 | async-start | bytes 2359296 | tf_op jit(solution)/shard_map/all_gather | solution.py:104
  7.9 152.9 %all-gather.10.cloned.1.call-start = ((), (), s32[]{:S(2)}) async-start(), calls=%async_computation.4 | async-start | bytes 4718592 | tf_op jit(solution)/shard_map/all_gather | solution.py:105
  8.6 165.9 %all-gather.6.cloned.1.call-start = ((), (), s32[]{:S(2)}) async-start(), calls=%async_computation.2 | async-start | bytes 6291456 | tf_op jit(solution)/shard_map/all_gather | solution.py:100
  10.5 81.0 %copy-start.5 = (f32[4,256,2,8]{1,3,2,0:T(8,128)S(1)}, f32[4,256,2,8]{1,3,2,0:T(8,128)}, u32[]{:S(2)}) copy-start(f32[4,256,2,8]{1,3,2,0:T(8,128)} %param.19) | copy-start | bytes 196612
  10.5 85.3 %copy-start.6 = (bf16[4,2048]{1,0:T(4,128)(2,1)S(1)}, bf16[4,2048]{1,0:T(4,128)(2,1)}, u32[]{:S(2)}) copy-start(bf16[4,2048]{1,0:T(4,128)(2,1)} %param.11) | copy-start | bytes 49156
  10.5 86.6 %copy-start.9 = (bf16[2048]{0:T(1024)(128)(2,1)S(1)}, bf16[2048]{0:T(1024)(128)(2,1)}, u32[]{:S(2)}) copy-start(bf16[2048]{0:T(1024)(128)(2,1)} %param.13) | copy-start | bytes 12292
  10.5 86.6 %copy-start.10 = (bf16[4,512]{1,0:T(4,128)(2,1)S(1)}, bf16[4,512]{1,0:T(4,128)(2,1)}, u32[]{:S(2)}) copy-start(bf16[4,512]{1,0:T(4,128)(2,1)} %param.12) | copy-start | bytes 12292
  10.5 86.7 %copy-start.7 = (bf16[2048,16]{0,1:T(8,128)(2,1)S(1)}, bf16[2048,16]{0,1:T(8,128)(2,1)}, u32[]{:S(2)}) copy-start(bf16[2048,16]{0,1:T(8,128)(2,1)} %param.17) | copy-start | bytes 196612
  10.5 86.7 %copy-start.8 = (bf16[2048,16]{0,1:T(8,128)(2,1)S(1)}, bf16[2048,16]{0,1:T(8,128)(2,1)}, u32[]{:S(2)}) copy-start(bf16[2048,16]{0,1:T(8,128)(2,1)} %param.16) | copy-start | bytes 196612
  92.2 87.1 %all-to-all-start.1 = ((f32[8,16,128]{2,1,0:T(8,128)}), f32[8,16,128]{2,1,0:T(8,128)S(1)}, u32[]{:S(2)}, u32[]{:S(2)}) async-start(f32[8,16,128]{2,1,0:T(8,128)} %copy.36), calls=%async_computation.1 | async-start | bytes 131072 | tf_op jit(solution)/shard_map/all_to_all | solution.py:102
  174.6 3.4 %copy-start = (bf16[1024,2048]{1,0:T(8,128)(2,1)S(1)}, bf16[1024,2048]{1,0:T(8,128)(2,1)}, u32[]{:S(2)}) copy-start(bf16[1024,2048]{1,0:T(8,128)(2,1)} %all-gather.6.cloned.1.call-done) | copy-start | bytes 12582916
  177.8 1.5 copy-start.11
  178.0 33.3 %copy-start.1 = (bf16[2048,512]{1,0:T(8,128)(2,1)S(1)}, bf16[2048,512]{1,0:T(8,128)(2,1)}, u32[]{:S(2)}) copy-start(bf16[2048,512]{1,0:T(8,128)(2,1)} %all-gather.8.cloned.1.call-done) | copy-start | bytes 6291460
  211.3 4.7 %copy-start.4 = (f32[8,1024]{1,0:T(8,128)}, f32[8,1024]{1,0:T(8,128)S(1)}, u32[]{:S(2)}) copy-start(f32[8,1024]{1,0:T(8,128)S(1)} %get-tuple-element.12) | copy-start | bytes 98308
  215.9 8.6 %copy-start.3 = (bf16[1024,512]{1,0:T(8,128)(2,1)}, bf16[1024,512]{1,0:T(8,128)(2,1)S(1)}, u32[]{:S(2)}) copy-start(bf16[1024,512]{1,0:T(8,128)(2,1)S(1)} %multiply_convert_fusion) | copy-start | bytes 3145732
  224.5 32.4 %copy-start.2 = (bf16[1024,1024]{1,0:T(8,128)(2,1)}, bf16[1024,1024]{1,0:T(8,128)(2,1)S(1)}, u32[]{:S(2)}) copy-start(bf16[1024,1024]{1,0:T(8,128)(2,1)S(1)} %convolution_convert_fusion) | copy-start | bytes 6291460
Sparse Core Ops, SparseCore 0:
  10.1 76.4 all-gather.7
  88.7 72.0 all-gather.9
  162.3 12.1 all-gather.5

commit v2 on v1

--- a/solution.py
+++ b/solution.py
@@ -1,6 +1,10 @@
+import functools
+
 import jax
 import jax.numpy as jnp
 from jax import lax
+from jax.experimental import pallas as pl
+from jax.experimental.pallas import tpu as pltpu
 from jax.sharding import PartitionSpec as P
 
 EPSILON = 1e-06
@@ -71,6 +75,352 @@
     return total / jnp.maximum(jnp.abs(weight), 1.0)[..., None]
 
 
+def line_width(group):
+    width = 1
+    while width * width * 4 <= group:
+        width *= 2
+    return width
+
+
+def move_and_project(
+    sizes,
+    tokens,
+    weight,
+    offsets,
+    new_rows,
+    norm_gain,
+    gate_weight,
+    keys_out,
+    values_out,
+    gates_out,
+    offsets_out,
+    fresh_out,
+    held_weight,
+    held_tokens,
+    normed,
+    local_sem,
+    z_send,
+    z_recv,
+    y_send,
+    y_recv,
+    x_send,
+    x_recv,
+    t_send,
+    t_recv,
+    f_send,
+    f_recv,
+    o_send,
+    o_recv,
+):
+    depth, width, groups, shares, scale = sizes
+    group = depth * width
+    sub, model_width = tokens.shape[1:]
+    part = model_width // shares
+    x, s, c = lax.axis_index("gr"), lax.axis_index("sp"), lax.axis_index("tp")
+    z, y = s // width, s % width
+
+    def wrap(value, size):
+        return lax.rem(value, size)
+
+    barrier = pltpu.get_barrier_semaphore()
+    partners = [{"sp": wrap(s + k, group)} for k in range(1, group)]
+    partners += [{"gr": wrap(x + k, groups)} for k in range(1, groups)]
+    partners += [{"tp": wrap(c + k, shares)} for k in range(1, shares)]
+    for partner in partners:
+        pl.semaphore_signal(barrier, inc=1, device_id=partner, device_id_type=pl.DeviceIdType.MESH)
+    pl.semaphore_wait(barrier, len(partners))
+
+    def remote(src, dst, send, recv, to):
+        return pltpu.make_async_remote_copy(
+            src_ref=src,
+            dst_ref=dst,
+            send_sem=send,
+            recv_sem=recv,
+            device_id=to,
+            device_id_type=pl.DeviceIdType.MESH,
+        )
+
+    def piece(zz, yy, xx, own=False):
+        return weight.at[xx] if own else held_weight.at[zz * width + yy, xx]
+
+    def along_z(zz, way, own=False):
+        return remote(
+            piece(zz, y, x, own),
+            held_weight.at[zz * width + y, x],
+            z_send.at[zz, way],
+            z_recv.at[zz],
+            {"sp": s + (width if way else -width)},
+        )
+
+    def along_y(zz, k, own=False):
+        return remote(
+            piece(zz, y, x, own),
+            held_weight.at[zz * width + y, x],
+            y_send.at[zz, k],
+            y_recv.at[zz, y],
+            {"sp": z * width + wrap(y + k, width)},
+        )
+
+    def along_x(zz, yy, k):
+        return remote(
+            held_weight.at[zz * width + yy, x],
+            held_weight.at[zz * width + yy, x],
+            x_send.at[zz * width + yy, k],
+            x_recv.at[zz * width + yy, x],
+            {"gr": wrap(x + k, groups)},
+        )
+
+    def got_z(zz):
+        ref = held_weight.at[zz * width + y, x]
+        remote(ref, ref, z_send.at[zz, 0], z_recv.at[zz], {"sp": s}).wait_recv()
+
+    def got_y(zz, yy):
+        ref = held_weight.at[zz * width + yy, x]
+        remote(ref, ref, y_send.at[zz, 0], y_recv.at[zz, yy], {"sp": s}).wait_recv()
+
+    def got_x(ss, xx):
+        ref = held_weight.at[ss, xx]
+        remote(ref, ref, x_send.at[ss, 0], x_recv.at[ss, xx], {"sp": s}).wait_recv()
+
+    columns = pl.ds(pl.multiple_of(c * part, part), part)
+
+    def send_block(to):
+        return remote(
+            tokens.at[to, :, columns],
+            held_tokens.at[s, :, columns],
+            t_send.at[to],
+            t_recv.at[s],
+            {"sp": to},
+        )
+
+    def send_offsets(to):
+        return remote(
+            offsets.at[to], offsets_out.at[s], o_send.at[to], o_recv.at[s], {"sp": to}
+        )
+
+    def forward_block(source, k):
+        return remote(
+            held_tokens.at[source, :, columns],
+            held_tokens.at[source, :, columns],
+            f_send.at[source, k],
+            f_recv.at[source, c],
+            {"tp": wrap(c + k, shares)},
+        )
+
+    def got_block(source):
+        ref = held_tokens.at[source, :, columns]
+        remote(ref, ref, t_send.at[source], t_recv.at[source], {"sp": s}).wait_recv()
+
+    def got_forward(source, k):
+        cc = wrap(c + k, shares)
+        at = pl.ds(pl.multiple_of(cc * part, part), part)
+        ref = held_tokens.at[source, :, at]
+        remote(ref, ref, f_send.at[source, 0], f_recv.at[source, cc], {"sp": s}).wait_recv()
+
+    def got_offsets(source):
+        ref = offsets_out.at[source]
+        remote(ref, ref, o_send.at[source], o_recv.at[source], {"sp": s}).wait_recv()
+
+    def sides(d, body):
+        for way in (1, 0):
+            zz = z - d if way else z + d
+            pl.when((zz >= 0) & (zz < depth))(functools.partial(body, zz, way))
+
+    def z_onward(zz, way, run, own=False):
+        there = z + (1 if way else -1)
+
+        @pl.when((there >= 0) & (there < depth))
+        def _():
+            run(along_z(zz, way, own))
+
+    start = lambda copy: copy.start()
+
+    def tokens_at(distance, run):
+        def one(zz, way):
+            for k in range(width):
+                run(zz * width + wrap(y + k, width))
+
+        if distance:
+            sides(distance, one)
+        else:
+            for k in range(1, width):
+                run(z * width + wrap(y + k, width))
+
+    own_weight = pltpu.make_async_copy(weight, held_weight.at[s], local_sem.at[0])
+    own_tokens = pltpu.make_async_copy(tokens.at[s], held_tokens.at[s], local_sem.at[1])
+    own_offsets = pltpu.make_async_copy(offsets.at[s], offsets_out.at[s], local_sem.at[2])
+    for way in (1, 0):
+        z_onward(z, way, start, True)
+    for k in range(1, width):
+        along_y(z, k, True).start()
+    for k in range(1, group):
+        send_offsets(wrap(s + k, group)).start()
+    own_weight.start()
+    own_tokens.start()
+    own_offsets.start()
+    tokens_at(0, lambda to: send_block(to).start())
+
+    def y_pieces(zz, way):
+        for k in range(1, width):
+            yy = wrap(y + k, width)
+            got_y(zz, yy)
+            for kk in range(1, groups):
+                along_x(zz, yy, kk).start()
+
+    def z_pieces(zz, way):
+        got_z(zz)
+        z_onward(zz, way, start)
+        for k in range(1, width):
+            along_y(zz, k).start()
+        for k in range(1, groups):
+            along_x(zz, y, k).start()
+
+    for d in range(1, depth):
+        sides(d, z_pieces)
+        tokens_at(depth - d, lambda to: send_block(to).start())
+        if d == 1:
+            y_pieces(z, 1)
+        else:
+            sides(d - 1, y_pieces)
+    sides(depth - 1, y_pieces)
+
+    def norm(rows):
+        wide = rows.astype(jnp.float32)
+        mean = jnp.mean(wide * wide, axis=-1, keepdims=True)
+        gain = norm_gain[...].astype(jnp.float32)
+        return (wide * lax.rsqrt(mean + EPSILON) * gain).astype(jnp.bfloat16)
+
+    def norm_block(source):
+        at = pl.ds(pl.multiple_of(source * sub, sub), sub)
+        normed[at, :] = norm(held_tokens[source])
+
+    def order(body):
+        tokens_at(0, body)
+        for d in range(depth - 1, 0, -1):
+            tokens_at(d, body)
+
+    fresh = norm(new_rows[...])
+    own_tokens.wait()
+    norm_block(s)
+
+    def pass_on(source):
+        got_block(source)
+        for k in range(1, shares):
+            forward_block(source, k).start()
+
+    def take(source):
+        for k in range(1, shares):
+            got_forward(source, k)
+        norm_block(source)
+
+    order(pass_on)
+    order(take)
+    own_weight.wait()
+    for k in range(1, group):
+        for kk in range(1, groups):
+            got_x(wrap(s + k, group), wrap(x + kk, groups))
+
+    key_columns, value_columns = keys_out.shape[1], values_out.shape[1]
+    rows = normed.shape[0]
+    tall = min(rows, 512)
+
+    gates_out[...] = jnp.dot(normed[...], gate_weight[...], preferred_element_type=jnp.float32)
+    total = key_columns + value_columns
+    fresh_out[:, total:] = jnp.dot(fresh, gate_weight[...], preferred_element_type=jnp.float32)
+
+    def project(out, first, factor):
+        wide = 256 if out.shape[1] % 256 == 0 else 128
+
+        @pl.loop(0, out.shape[1] // wide)
+        def _(n):
+            at = pl.ds(pl.multiple_of(n * wide, wide), wide)
+            from_at = pl.ds(pl.multiple_of(first + n * wide, wide if first % wide == 0 else 128), wide)
+            w = held_weight[:, :, :, from_at].reshape(model_width, wide)
+            new = jnp.dot(fresh, w, preferred_element_type=jnp.float32)
+            fresh_out[:, from_at] = new * factor
+            for m in range(rows // tall):
+                lines = pl.ds(m * tall, tall)
+                got = jnp.dot(normed[lines, :], w, preferred_element_type=jnp.float32)
+                out[lines, at] = (got * factor).astype(out.dtype)
+
+    project(keys_out, 0, scale)
+    project(values_out, key_columns, 1.0)
+
+    own_offsets.wait()
+    for k in range(1, group):
+        got_offsets(wrap(s + k, group))
+
+    for way in (1, 0):
+        z_onward(z, way, lambda copy: copy.wait_send(), True)
+    for k in range(1, width):
+        along_y(z, k, True).wait_send()
+    for k in range(1, group):
+        to = wrap(s + k, group)
+        send_offsets(to).wait_send()
+        send_block(to).wait_send()
+        for kk in range(1, shares):
+            forward_block(to, kk).wait_send()
+        for kk in range(1, groups):
+            along_x(to // width, to % width, kk).wait_send()
+
+    def sent_z(zz, way):
+        z_onward(zz, way, lambda copy: copy.wait_send())
+        for k in range(1, width):
+            along_y(zz, k).wait_send()
+
+    for d in range(1, depth):
+        sides(d, sent_z)
+
+
+def gather_and_project(tokens, weight, offsets, new_rows, norm_gain, gate_weight, key_columns, scale):
+    group, sub, model_width = tokens.shape
+    width = line_width(group)
+    depth = group // width
+    groups, shares = lax.axis_size("gr"), lax.axis_size("tp")
+    total = weight.shape[1]
+    rows = group * sub
+    sizes = (depth, width, groups, shares, scale)
+    share = weight.shape[0] // groups
+    dma = pltpu.SemaphoreType.DMA
+    vmem = pl.BlockSpec(memory_space=pltpu.VMEM)
+    hbm = pl.BlockSpec(memory_space=pl.ANY)
+    lanes = gate_weight.shape[1]
+    return pl.pallas_call(
+        functools.partial(move_and_project, sizes),
+        name="move_and_project",
+        out_shape=(
+            jax.ShapeDtypeStruct((rows, key_columns), jnp.bfloat16),
+            jax.ShapeDtypeStruct((rows, total - key_columns), jnp.bfloat16),
+            jax.ShapeDtypeStruct((rows, lanes), jnp.float32),
+            jax.ShapeDtypeStruct(offsets.shape, jnp.float32),
+            jax.ShapeDtypeStruct((new_rows.shape[0], total + lanes), jnp.float32),
+        ),
+        in_specs=[hbm, hbm, hbm, vmem, vmem, vmem],
+        out_specs=(vmem, vmem, vmem, vmem, vmem),
+        scratch_shapes=[
+            pltpu.VMEM((group, groups, share, total), jnp.bfloat16),
+            pltpu.VMEM((group, sub, model_width), jnp.bfloat16),
+            pltpu.VMEM((rows, model_width), jnp.bfloat16),
+            dma((3,)),
+            dma((depth, 2)),
+            dma((depth,)),
+            dma((depth, width)),
+            dma((depth, width)),
+            dma((group, groups)),
+            dma((group, groups)),
+            dma((group,)),
+            dma((group,)),
+            dma((group, shares)),
+            dma((group, shares)),
+            dma((group,)),
+            dma((group,)),
+        ],
+        compiler_params=pltpu.CompilerParams(
+            collective_id=0, has_side_effects=True, vmem_limit_bytes=48 * 1024 * 1024
+        ),
+    )(tokens, weight.reshape(groups, share, total), offsets, new_rows, norm_gain, gate_weight)
+
+
 def per_device(
     tokens,
     new_rows,
@@ -87,25 +437,14 @@
     heads = forget_bias.shape[0]
     key_size = key_weight.shape[1] // heads
     group = lax.axis_size("sp")
-    shares = lax.axis_size("tp")
     pieces = group // seq_count
     sub = positions // pieces
     rows = group * sub
     index, core = lax.axis_index("sp"), lax.axis_index("tp")
     prompt = index // pieces
 
-    part = model_width // shares
-    mine = lax.dynamic_slice_in_dim(tokens.reshape(group, sub, model_width), core * part, part, 2)
-    moved = lax.all_to_all(mine, "sp", split_axis=0, concat_axis=0, tiled=True)
-    source = lax.all_gather(moved.reshape(rows, part), "tp", axis=1, tiled=True)
     offsets = jnp.transpose(gate_offsets.reshape(group, sub, 2 * heads), (0, 2, 1))
-    offsets = lax.all_to_all(offsets, "sp", split_axis=0, concat_axis=0, tiled=True)
-    offsets = jnp.transpose(offsets, (1, 0, 2)).reshape(2 * heads, rows)
-    key_weight = lax.all_gather(key_weight, "sp", axis=0, tiled=True)
-    value_weight = lax.all_gather(value_weight, "sp", axis=0, tiled=True)
-
-    normed = normed_rows(source, norm_gain)
-    fresh = normed_rows(lax.dynamic_slice_in_dim(new_rows, prompt, 1, 0), norm_gain)
+    weight = jnp.concatenate([key_weight, value_weight], axis=1)
     head_start = core * heads
     gate_weight = jnp.concatenate(
         [
@@ -113,17 +452,26 @@
             lax.dynamic_slice_in_dim(forget_weight, head_start, heads, 1),
         ],
         axis=1,
-    ).T
-    gates = contract_last(gate_weight, normed)
-    gate_new = contract_last(gate_weight[:heads], fresh)
-
-    def project(x):
-        keys = jnp.dot(x, key_weight, preferred_element_type=jnp.float32) * key_size**-0.5
-        values = jnp.dot(x, value_weight, preferred_element_type=jnp.float32)
-        return keys.astype(jnp.bfloat16), values.astype(jnp.bfloat16)
-
-    keys, values = project(normed)
-    key_new, value_new = project(fresh)
+    )
+    gate_weight = jnp.pad(gate_weight, ((0, 0), (0, -2 * heads % 128)))
+    key_columns = key_weight.shape[1]
+    keys, values, gates, offsets, fresh = gather_and_project(
+        tokens.reshape(group, sub, model_width),
+        weight,
+        offsets,
+        jnp.pad(new_rows, ((0, -seq_count % 16), (0, 0))),
+        norm_gain[None],
+        gate_weight,
+        key_columns,
+        key_size**-0.5,
+    )
+    gates = gates[:, : 2 * heads].T
+    offsets = jnp.transpose(offsets, (1, 0, 2)).reshape(2 * heads, rows)
+    fresh = lax.dynamic_slice_in_dim(fresh, prompt, 1, 0)
+    total = weight.shape[1]
+    key_new = fresh[:, :key_columns].astype(jnp.bfloat16)
+    value_new = fresh[:, key_columns:total].astype(jnp.bfloat16)
+    gate_new = fresh[:, total : total + heads].reshape(heads, 1)
     log_weight = log_weights(gates, offsets, forget_bias, heads, group, pieces)
     query = lax.dynamic_slice_in_dim(new_query, prompt, 1, 0)
     peak, numerator, denominator = read_part(query, keys, values, log_weight, heads)

time: 264 us -> 180 us (0.68)
  Pallas kernels: 0 us -> 91.6 us
  blocking collectives: 142 us -> 61.1 us
  waiting for transfers between devices: 73.4 us -> 0 us
  matrix products: 19.9 us -> 3.91 us
  between operations: 14.8 us -> 0.86 us
  local copies, waits for them, and re-layouts: 3.73 us -> 15 us
  starting transfers between devices: 3.71 us -> 0 us
    pallas_call x0 -> x1, Pallas kernels: none -> 91.6 us  [gather_and_project(): pl.pallas_call(functools.partial(move_and_project, sizes), name='move_and...]
    all_to_all x1 -> x0, blocking collectives: 80.9 us -> none  [per_device(): moved = lax.all_to_all(mine, 'sp', split_axis=0, concat_axis=0, tiled=True)]
    all_gather x3 -> x0, waiting for transfers between devices: 72 us -> none  [the longest x1 61.1 us: per_device(): value_weight = lax.all_gather(value_weight, 'sp', axis=0, tiled=True)]
    dot_general x4 -> x0, matrix products: 17.4 us -> none  [the longest x2 10.8 us: project(): values = jnp.dot(x, value_weight, preferred_element_type=jnp.float32)]
    unnamed x30, local copies, waits for them, and re-layouts: 0.6 us -> 8.15 us
    reduce_sum x3 -> x0, other arithmetic: 3.93 us -> none  [the longest x2 3.84 us: normed_rows(): jnp.mean(widened * widened, axis=-1, keepdims=True) + EPSILON]
    all_to_all x1 -> x0, starting transfers between devices: 3.59 us -> none  [per_device(): lax.all_to_all(offsets, 'sp', split_axis=0, concat_axis=0, tiled=True)]
  transfers between devices with their start and end apart: 4 -> 0, of which waited for: 2 -> 0; matrix products, arithmetic and copies ran while one was open for 5% -> 0% of each run, Pallas kernels for 0% -> 0%
where the time goes in v2:
time: 180 us; the launch traced here: 179 us
  Pallas kernels  91.6 us (51%)
  blocking collectives  61.1 us (34%)
  local copies, waits for them, and re-layouts  15 us (8%)
  other arithmetic  6.93 us (4%)
  matrix products  3.91 us (2%)
    pallas_call x1, Pallas kernels, gather_and_project(): pl.pallas_call(functools.partial(move_and_project, sizes), name='move_and...  91.6 us
    all_gather x1, blocking collectives, log_weights(): everything = lax.all_gather(totals, 'sp')  30.6 us
    all_gather x1, blocking collectives, finish(): lax.all_gather(packed, 'sp').reshape(seq_count, pieces, heads, -1)  30.6 us
    unnamed x30, local copies, waits for them, and re-layouts  8.15 us

profile of v2, /device:TPU:0, one launch (start us, length us, event | category | flops | bytes accessed | tf_op | source)
XLA Modules:
  0.0 179.4 jit_solution(6567488731348173750)
XLA Ops:
  0.6 0.0 copy-start.5
  0.6 0.0 copy-start.4
  0.7 0.0 copy-start.6
  0.7 0.0 copy-start.7
  0.7 0.0 copy-start.8
  0.7 0.8 constant_dynamic-slice_fusion.1
  1.6 0.3 copy.81
  1.9 0.9 pad.13.gate_weight
  2.8 0.0 copy-done.5
  2.8 0.0 copy-done.4
  2.8 0.9 pad_maximum_fusion
  3.7 0.0 copy-done.6
  3.8 0.0 copy-done.7
  3.8 0.0 copy-done.8
  3.9 0.0 copy-start
  3.9 1.1 copy-done
  5.0 0.0 copy-start.1
  5.0 1.0 copy-done.1
  6.0 0.0 copy-start.10
  6.0 91.6 %move_and_project.1 = (bf16[1024,512]{1,0:T(8,128)(2,1)S(1)}, bf16[1024,1024]{1,0:T(8,128)(2,1)S(1)}, f32[1024,128]{1,0:T(8,128)S(1)}, f32[8,16,128]{2,1,0:T(8,128)S(1)}, f32[16,1664]{1,0:T(8,128)S(1)}) custom-call(bf16[8,128,2048]{2,1,0:T(8,128)(2,1)} %bitcast.77, bf16[2,128,1536]{2,1,0:T(8,128)(2,1)S(1)} %bitcast.73, f32[8,16,128]{2,1,0:T(8,128)S(1)} %bitcast.74, ...), custom_call_target="tpu_custom_call" | custom-call | tf_op jit(solution)/shard_map/move_and_project/pallas_call | solution.py:388
  97.7 0.0 copy-start.2
  97.7 0.8 copy-done.2
  98.5 1.0 copy.84
  99.5 1.1 slice_bitcast_fusion
  100.5 0.0 copy-start.3
  100.5 0.8 copy-done.3
  101.3 0.0 copy-done.10
  101.3 2.3 %bitcast_reduce_fusion = (f32[8,8]{0,1:T(8,128)S(1)}, f32[8,1024]{0,1:T(8,128)}) fusion(f32[8,1024]{0,1:T(8,128)} %copy.84, f32[8]{0:T(128)S(1)} %copy-done.10, f32[16,1024]{0,1:T(8,128)S(1)} %slice_bitcast_fusion), kind=kLoop, calls=%fused_computation.75 | loop fusion | flops 90048 | bytes 98592 | tf_op jit(solution)/shard_map/reduce_sum | solution.py:32
  103.6 0.0 copy-start.9
  103.6 0.1 copy.86
  103.7 30.6 %all-gather = f32[64,8]{1,0:T(8,128)S(1)} all-gather(f32[8,8]{1,0:T(8,128)S(1)} %copy.86), channel_id=2, replica_groups=mesh['gr'=2,'sp'=8,'tp'=2] {'sp'}, dimensions={0}, use_global_device_ids=true | all-gather | bytes 2304 | tf_op jit(solution)/shard_map/all_gather | solution.py:34
  134.3 0.1 dynamic-slice_reduce_fusion
  134.4 0.1 rev.7
  134.4 0.2 reduce_window_sum.11
  134.6 0.1 rev.8
  134.7 0.1 copy.87
  134.8 2.0 %convolution_add_fusion = f32[8,8,128]{2,0,1:T(8,128)S(1)} fusion(f32[8,8,128]{0,2,1:T(8,128)} %bitcast.78, s32[128]{0:T(128)S(1)} %iota_add_fusion, f32[8,8]{0,1:T(8,128)S(1)} %copy.87), kind=kOutput, calls=%fused_computation.4 | convolution fusion | flops 12623872 | bytes 66304 | tf_op jit(solution)/shard_map/dot_general | solution.py:31
  136.8 1.0 copy.88
  137.8 1.0 copy.82
  138.8 2.2 %fusion.30 = (f32[8]{0:T(128)S(1)}, f32[8,1024]{0,1:T(8,128)}) fusion(f32[8,8,128]{0,2,1:T(8,128)} %copy.88, f32[8,1024]{0,1:T(8,128)} %copy.82, f32[16,1024]{0,1:T(8,128)} %copy-done.3), kind=kLoop, calls=%fused_computation.79 | loop fusion | flops 24568 | bytes 131104 | tf_op jit(solution)/shard_map/reduce_max | solution.py:48
  141.0 0.0 copy-done.9
  141.1 1.5 fusion.33
  142.5 0.4 fusion.1
  143.0 0.1 reshape.149
  143.1 0.1 reduce_sum.79
  143.2 0.1 dynamic-slice_bitcast_fusion
  143.3 0.1 copy.94
  143.4 30.6 %all-gather.1 = f32[64,384]{1,0:T(8,128)S(1)} all-gather(f32[8,384]{1,0:T(8,128)S(1)} %select_maximum_fusion), channel_id=3, replica_groups=mesh['gr'=2,'sp'=8,'tp'=2] {'sp'}, dimensions={0}, use_global_device_ids=true | all-gather | bytes 110592 | tf_op jit(solution)/shard_map/all_gather | solution.py:64
  173.9 0.2 slice_reduce_fusion.3
  174.1 0.1 slice_reduce_fusion.2
  174.2 0.2 exponential_reduce_fusion
  174.4 0.1 fusion.9
  174.5 0.1 broadcast_bitcast_fusion
  174.6 0.1 broadcast_bitcast_fusion.1
  174.7 0.6 fusion.15
  175.3 1.8 %copy.91 = f32[1,8,1024]{2,1,0:T(8,128)} copy(f32[1,8,1024]{1,2,0:T(8,128)} %bitcast.76) | data formatting | bytes 65536
  177.1 1.0 copy.115
  178.1 1.3 copy.116
  (22 shorter events, 0.3 us)
Async XLA Ops:
  0.6 2.1 %copy-start.5 = (bf16[256,512]{1,0:T(8,128)(2,1)S(1)}, bf16[256,512]{1,0:T(8,128)(2,1)}, u32[]{:S(2)}) copy-start(bf16[256,512]{1,0:T(8,128)(2,1)} %param.14) | copy-start | bytes 786436
  0.6 2.1 %copy-start.4 = (bf16[256,1024]{1,0:T(8,128)(2,1)S(1)}, bf16[256,1024]{1,0:T(8,128)(2,1)}, u32[]{:S(2)}) copy-start(bf16[256,1024]{1,0:T(8,128)(2,1)} %param.15) | copy-start | bytes 1572868
  0.7 3.0 %copy-start.6 = (f32[4,256,2,8]{1,3,2,0:T(8,128)S(1)}, f32[4,256,2,8]{1,3,2,0:T(8,128)}, u32[]{:S(2)}) copy-start(f32[4,256,2,8]{1,3,2,0:T(8,128)} %param.19) | copy-start | bytes 196612
  0.7 3.1 %copy-start.7 = (bf16[4,2048]{1,0:T(4,128)(2,1)S(1)}, bf16[4,2048]{1,0:T(4,128)(2,1)}, u32[]{:S(2)}) copy-start(bf16[4,2048]{1,0:T(4,128)(2,1)} %param.11) | copy-start | bytes 49156
  0.7 3.2 %copy-start.8 = (bf16[2048]{0:T(1024)(128)(2,1)S(1)}, bf16[2048]{0:T(1024)(128)(2,1)}, u32[]{:S(2)}) copy-start(bf16[2048]{0:T(1024)(128)(2,1)} %param.13) | copy-start | bytes 12292
  3.9 1.1 copy-start
  5.0 1.0 copy-start.1
  6.0 95.3 %copy-start.10 = (f32[8]{0:T(128)S(1)}, f32[8]{0:T(128)}, u32[]{:S(2)}) copy-start(f32[8]{0:T(128)} %param.18) | copy-start | bytes 100
  97.7 0.8 copy-start.2
  100.5 0.8 copy-start.3
  103.6 37.4 %copy-start.9 = (bf16[4,512]{1,0:T(4,128)(2,1)S(1)}, bf16[4,512]{1,0:T(4,128)(2,1)}, u32[]{:S(2)}) copy-start(bf16[4,512]{1,0:T(4,128)(2,1)} %param.12) | copy-start | bytes 12292

commit v3 on v2

--- a/solution.py
+++ b/solution.py
@@ -19,6 +19,53 @@
 
 def contract_last(a, b):
     return lax.dot_general(a, b, (((1,), (1,)), ((), ())), preferred_element_type=jnp.float32)
+
+
+def exchange_kernel(group, mine, everyone, send, recv, local):
+    s = lax.axis_index("sp")
+    mesh_id = pl.DeviceIdType.MESH
+    barrier = pltpu.get_barrier_semaphore()
+    for k in range(1, group):
+        to = {"sp": lax.rem(s + k, group)}
+        pl.semaphore_signal(barrier, inc=1, device_id=to, device_id_type=mesh_id)
+    own = pltpu.make_async_copy(mine, everyone.at[s], local)
+    own.start()
+    pl.semaphore_wait(barrier, group - 1)
+
+    def copy(k, slot):
+        return pltpu.make_async_remote_copy(
+            src_ref=mine,
+            dst_ref=everyone.at[slot],
+            send_sem=send.at[k],
+            recv_sem=recv.at[slot],
+            device_id={"sp": lax.rem(s + k, group)},
+            device_id_type=mesh_id,
+        )
+
+    for k in range(1, group):
+        copy(k, s).start()
+    for k in range(1, group):
+        copy(k, lax.rem(s + k, group)).wait_recv()
+    for k in range(1, group):
+        copy(k, s).wait_send()
+    own.wait()
+
+
+def gather_small(mine, name, number):
+    group = lax.axis_size("sp")
+    return pl.pallas_call(
+        functools.partial(exchange_kernel, group),
+        name=name,
+        out_shape=jax.ShapeDtypeStruct((group,) + mine.shape, mine.dtype),
+        in_specs=[pl.BlockSpec(memory_space=pl.ANY)],
+        out_specs=pl.BlockSpec(memory_space=pl.ANY),
+        scratch_shapes=[
+            pltpu.SemaphoreType.DMA((group,)),
+            pltpu.SemaphoreType.DMA((group,)),
+            pltpu.SemaphoreType.DMA,
+        ],
+        compiler_params=pltpu.CompilerParams(collective_id=number, has_side_effects=True),
+    )(mine)
 
 
 def log_weights(gates, offsets, forget_bias, heads, blocks, pieces):
@@ -31,7 +78,7 @@
     within = jnp.dot(by_block.reshape(heads * blocks, sub), later, precision=HIGHEST)
     totals = jnp.sum(by_block, axis=2)
     index = lax.axis_index("sp")
-    everything = lax.all_gather(totals, "sp")
+    everything = gather_small(totals, "gather_totals", 1)
     ours = lax.dynamic_slice_in_dim(everything, index // pieces * pieces, pieces, 0)
     piece = index % pieces
     all_pieces = jnp.sum(ours, axis=0)
@@ -61,7 +108,7 @@
     one = jnp.concatenate([peak, denominator, own_score, gate_new], axis=1)
     one = jnp.pad(one, ((0, 0), (0, value_size - one.shape[1])))
     packed = jnp.concatenate([numerator, value_new, one], axis=1)
-    everything = lax.all_gather(packed, "sp").reshape(seq_count, pieces, heads, -1)
+    everything = gather_small(packed, "gather_read", 2).reshape(seq_count, pieces, heads, -1)
     one = everything[..., 2 * value_size :]
     peaks, denominators = one[..., 0], one[..., 1]
     own_score, gate_new = one[:, 0, :, 2], one[:, 0, :, 3]

time: 180 us -> 138 us (0.77)
  blocking collectives: 61.1 us -> 0 us
  Pallas kernels: 91.6 us -> 105 us
  other arithmetic: 6.93 us -> 9.71 us
  local copies, waits for them, and re-layouts: 15 us -> 17.7 us
    all_gather x2 -> x0, blocking collectives: 61.1 us -> none  [the longest x1 30.6 us: log_weights(): everything = lax.all_gather(totals, 'sp')]
    pallas_call x0 -> x2, Pallas kernels: none -> 13.7 us  [gather_small(): pl.pallas_call(functools.partial(exchange_kernel, group), name=name, out_...]
    unnamed x30 -> x33, local copies, waits for them, and re-layouts: 8.15 us -> 9.23 us
where the time goes in v3:
time: 138 us; the launch traced here: 137 us
  Pallas kernels  105 us (76%)
  local copies, waits for them, and re-layouts  17.7 us (13%)
  other arithmetic  9.71 us (7%)
  matrix products  3.91 us (3%)
    pallas_call x1, Pallas kernels, gather_and_project(): pl.pallas_call(functools.partial(move_and_project, sizes), name='move_and...  91.6 us
    pallas_call x2, Pallas kernels, gather_small(): pl.pallas_call(functools.partial(exchange_kernel, group), name=name, out_...  13.7 us
    unnamed x33, local copies, waits for them, and re-layouts  9.23 us

profile of v3, /device:TPU:0, one launch (start us, length us, event | category | flops | bytes accessed | tf_op | source)
XLA Modules:
  0.0 137.4 jit_solution(10742926303772870149)
XLA Ops:
  0.6 0.0 copy-start.5
  0.6 0.0 copy-start.4
  0.7 0.0 copy-start.6
  0.7 0.0 copy-start.7
  0.7 0.0 copy-start.8
  0.7 0.8 constant_dynamic-slice_fusion.1
  1.6 0.3 copy.85
  1.9 0.9 pad.13.gate_weight
  2.8 0.0 copy-done.5
  2.8 0.0 copy-done.4
  2.8 0.9 pad_maximum_fusion
  3.7 0.0 copy-done.6
  3.8 0.0 copy-done.7
  3.8 0.0 copy-done.8
  3.9 0.0 copy-start
  3.9 1.1 copy-done
  5.0 1.0 copy-done.1
  6.0 91.6 %move_and_project.1 = (bf16[1024,512]{1,0:T(8,128)(2,1)S(1)}, bf16[1024,1024]{1,0:T(8,128)(2,1)S(1)}, f32[1024,128]{1,0:T(8,128)S(1)}, f32[8,16,128]{2,1,0:T(8,128)S(1)}, f32[16,1664]{1,0:T(8,128)S(1)}) custom-call(bf16[8,128,2048]{2,1,0:T(8,128)(2,1)} %bitcast.101, bf16[2,128,1536]{2,1,0:T(8,128)(2,1)S(1)} %bitcast.97, f32[8,16,128]{2,1,0:T(8,128)S(1)} %bitcast.98, ...), custom_call_target="tpu_custom_call" | custom-call | tf_op jit(solution)/shard_map/move_and_project/pallas_call | solution.py:435
  97.7 0.0 copy-start.2
  97.7 0.8 copy-done.2
  98.5 1.0 copy.88
  99.5 1.1 slice_bitcast_fusion
  100.5 0.0 copy-start.3
  100.5 0.8 copy-done.3
  101.3 0.0 copy-done.10
  101.3 2.3 %bitcast_reduce_fusion = (f32[8,8]{0,1:T(8,128)S(1)}, f32[8,1024]{0,1:T(8,128)}) fusion(f32[8,1024]{0,1:T(8,128)} %copy.88, f32[8]{0:T(128)S(1)} %copy-done.10, f32[16,1024]{0,1:T(8,128)S(1)} %slice_bitcast_fusion), kind=kLoop, calls=%fused_computation.78 | loop fusion | flops 90048 | bytes 98592 | tf_op jit(solution)/shard_map/reduce_sum | solution.py:79
  103.6 0.7 copy.90.mine
  104.3 6.8 %gather_totals.1 = f32[8,8,8]{2,1,0:T(8,128)} custom-call(f32[8,8]{1,0:T(8,128)} %copy.90.mine), custom_call_target="tpu_custom_call" | custom-call | tf_op jit(solution)/shard_map/gather_totals/pallas_call | solution.py:56
  111.1 0.8 dynamic-slice_reduce_fusion
  111.9 0.1 rev.7
  111.9 0.2 reduce_window_sum.11
  112.1 0.1 rev.8
  112.2 0.1 copy.91
  112.3 2.0 %convolution_add_fusion = f32[8,8,128]{2,0,1:T(8,128)S(1)} fusion(f32[8,8,128]{0,2,1:T(8,128)} %bitcast.102, s32[128]{0:T(128)S(1)} %iota_add_fusion, f32[8,8]{0,1:T(8,128)S(1)} %copy.91), kind=kOutput, calls=%fused_computation.4 | convolution fusion | flops 12623872 | bytes 66304 | tf_op jit(solution)/shard_map/dot_general | solution.py:78
  114.3 1.0 copy.92
  115.3 1.0 copy.86
  116.3 2.2 %fusion.33 = (f32[8]{0:T(128)S(1)}, f32[8,1024]{0,1:T(8,128)}) fusion(f32[8,8,128]{0,2,1:T(8,128)} %copy.92, f32[8,1024]{0,1:T(8,128)} %copy.86, f32[16,1024]{0,1:T(8,128)} %copy-done.3), kind=kLoop, calls=%fused_computation.83 | loop fusion | flops 24568 | bytes 131104 | tf_op jit(solution)/shard_map/reduce_max | solution.py:95
  118.5 0.0 copy-done.9
  118.6 1.5 %fusion.37 = (f32[8]{0:T(128)S(1)}, bf16[8,1024]{0,1:T(8,128)(2,1)S(1)}) fusion(bf16[1024,512]{1,0:T(8,128)(2,1)S(1)} %get-tuple-element.9, s32[512]{0:T(512)S(1)} %add_select_fusion, bf16[512]{0:T(512)(128)(2,1)S(1)} %fusion.29, f32[8,1024]{0,1:T(8,128)} %get-tuple-element.39, f32[8]{0:T(128)S(1)} %get-tuple-element.38), kind=kOutput, calls=%fused_computation.85 | convolution fusion | flops 8429560 | bytes 1100864 | tf_op jit(solution)/shard_map/dot_general | solution.py:21
  120.0 0.4 fusion.1
  120.4 0.1 copy.95
  120.5 0.1 copy.94
  120.7 0.1 reshape.149
  120.7 0.1 reduce_sum.79
  120.9 0.1 copy.96
  120.9 0.1 dynamic-slice_bitcast_fusion
  121.0 0.1 copy.97
  121.1 0.1 select_maximum_fusion
  121.2 0.6 pad_maximum_fusion.2.mine
  121.8 6.9 %gather_read.1 = f32[8,8,384]{2,1,0:T(8,128)} custom-call(f32[8,384]{1,0:T(8,128)} %pad_maximum_fusion.2.mine), custom_call_target="tpu_custom_call" | custom-call | tf_op jit(solution)/shard_map/gather_read/pallas_call | solution.py:56
  128.7 0.9 slice_reduce_fusion
  129.6 0.9 fusion.36
  130.5 0.1 copy.106
  130.6 0.1 copy.105
  130.7 0.8 fusion.9
  131.6 0.1 copy.108
  131.7 0.1 copy.107
  131.8 0.1 broadcast_bitcast_fusion
  131.9 0.1 broadcast_bitcast_fusion.1
  132.0 0.7 slice_bitcast_fusion.3
  132.7 0.6 fusion.15
  133.3 1.8 %copy.102 = f32[1,8,1024]{2,1,0:T(8,128)} copy(f32[1,8,1024]{1,2,0:T(8,128)} %bitcast.100) | data formatting | bytes 65536
  135.1 1.0 copy.130
  136.1 1.3 copy.131
  (23 shorter events, 0.3 us)
Async XLA Ops:
  0.6 2.1 %copy-start.5 = (bf16[256,512]{1,0:T(8,128)(2,1)S(1)}, bf16[256,512]{1,0:T(8,128)(2,1)}, u32[]{:S(2)}) copy-start(bf16[256,512]{1,0:T(8,128)(2,1)} %param.14) | copy-start | bytes 786436
  0.6 2.1 %copy-start.4 = (bf16[256,1024]{1,0:T(8,128)(2,1)S(1)}, bf16[256,1024]{1,0:T(8,128)(2,1)}, u32[]{:S(2)}) copy-start(bf16[256,1024]{1,0:T(8,128)(2,1)} %param.15) | copy-start | bytes 1572868
  0.7 3.0 %copy-start.6 = (f32[4,256,2,8]{1,3,2,0:T(8,128)S(1)}, f32[4,256,2,8]{1,3,2,0:T(8,128)}, u32[]{:S(2)}) copy-start(f32[4,256,2,8]{1,3,2,0:T(8,128)} %param.19) | copy-start | bytes 196612
  0.7 3.1 %copy-start.7 = (bf16[4,2048]{1,0:T(4,128)(2,1)S(1)}, bf16[4,2048]{1,0:T(4,128)(2,1)}, u32[]{:S(2)}) copy-start(bf16[4,2048]{1,0:T(4,128)(2,1)} %param.11) | copy-start | bytes 49156
  0.7 3.2 %copy-start.8 = (bf16[2048]{0:T(1024)(128)(2,1)S(1)}, bf16[2048]{0:T(1024)(128)(2,1)}, u32[]{:S(2)}) copy-start(bf16[2048]{0:T(1024)(128)(2,1)} %param.13) | copy-start | bytes 12292
  3.9 1.1 copy-start
  5.0 1.0 copy-start.1
  6.0 95.3 %copy-start.10 = (f32[8]{0:T(128)S(1)}, f32[8]{0:T(128)}, u32[]{:S(2)}) copy-start(f32[8]{0:T(128)} %param.18) | copy-start | bytes 100
  97.7 0.8 copy-start.2
  100.5 0.8 copy-start.3
  103.6 14.9 %copy-start.9 = (bf16[4,512]{1,0:T(4,128)(2,1)S(1)}, bf16[4,512]{1,0:T(4,128)(2,1)}, u32[]{:S(2)}) copy-start(bf16[4,512]{1,0:T(4,128)(2,1)} %param.12) | copy-start | bytes 12292

commit v4 on v3

--- a/solution.py
+++ b/solution.py
@@ -68,7 +68,7 @@
     )(mine)
 
 
-def log_weights(gates, offsets, forget_bias, heads, blocks, pieces):
+def log_weights(gates, offsets, forget_bias, totals, heads, blocks, pieces):
     rows = gates.shape[1]
     sub = rows // blocks
     input_gate = gates[:heads] + offsets[:heads]
@@ -76,9 +76,8 @@
     by_block = log_forget.reshape(heads, blocks, sub)
     later = jnp.tril(jnp.ones((sub, sub), jnp.float32), -1)
     within = jnp.dot(by_block.reshape(heads * blocks, sub), later, precision=HIGHEST)
-    totals = jnp.sum(by_block, axis=2)
     index = lax.axis_index("sp")
-    everything = gather_small(totals, "gather_totals", 1)
+    everything = totals[:, :, :blocks]
     ours = lax.dynamic_slice_in_dim(everything, index // pieces * pieces, pieces, 0)
     piece = index % pieces
     all_pieces = jnp.sum(ours, axis=0)
@@ -137,11 +136,13 @@
     new_rows,
     norm_gain,
     gate_weight,
+    forget_bias,
     keys_out,
     values_out,
     gates_out,
     offsets_out,
     fresh_out,
+    totals_out,
     held_weight,
     held_tokens,
     normed,
@@ -158,6 +159,8 @@
     f_recv,
     o_send,
     o_recv,
+    s_send,
+    s_recv,
 ):
     depth, width, groups, shares, scale = sizes
     group = depth * width
@@ -245,6 +248,10 @@
             offsets.at[to], offsets_out.at[s], o_send.at[to], o_recv.at[s], {"sp": to}
         )
 
+    def send_totals(to, slot):
+        ref = totals_out.at[slot]
+        return remote(ref, ref, s_send.at[to], s_recv.at[slot], {"sp": to})
+
     def forward_block(source, k):
         return remote(
             held_tokens.at[source, :, columns],
@@ -362,6 +369,23 @@
 
     order(pass_on)
     order(take)
+    own_offsets.wait()
+    for k in range(1, group):
+        got_offsets(wrap(s + k, group))
+
+    heads = forget_bias.shape[0]
+    gates = jnp.dot(normed[...], gate_weight[...], preferred_element_type=jnp.float32).T
+    gates_out[...] = gates[: gates_out.shape[0]]
+    lane = lax.broadcasted_iota(jnp.int32, (heads, totals_out.shape[2]), 1)
+    totals = jnp.zeros((heads, totals_out.shape[2]), jnp.float32)
+    for j in range(group):
+        pre = gates[heads : 2 * heads, j * sub : (j + 1) * sub] + forget_bias[...]
+        log_forget = jnp.minimum(pre, 0.0) - jnp.log1p(jnp.exp(-jnp.abs(pre)))
+        log_forget = log_forget + offsets_out[j, heads : 2 * heads, :]
+        block_total = jnp.sum(log_forget, axis=1, keepdims=True)
+        totals = totals + jnp.where(lane == j, block_total, 0.0)
+    totals_out[s] = totals
+
     own_weight.wait()
     for k in range(1, group):
         for kk in range(1, groups):
@@ -371,7 +395,8 @@
     rows = normed.shape[0]
     tall = min(rows, 512)
 
-    gates_out[...] = jnp.dot(normed[...], gate_weight[...], preferred_element_type=jnp.float32)
+    for k in range(1, group):
+        send_totals(wrap(s + k, group), s).start()
     total = key_columns + value_columns
     fresh_out[:, total:] = jnp.dot(fresh, gate_weight[...], preferred_element_type=jnp.float32)
 
@@ -393,9 +418,9 @@
     project(keys_out, 0, scale)
     project(values_out, key_columns, 1.0)
 
-    own_offsets.wait()
-    for k in range(1, group):
-        got_offsets(wrap(s + k, group))
+    for k in range(1, group):
+        other = wrap(s + k, group)
+        send_totals(other, other).wait_recv()
 
     for way in (1, 0):
         z_onward(z, way, lambda copy: copy.wait_send(), True)
@@ -404,6 +429,7 @@
     for k in range(1, group):
         to = wrap(s + k, group)
         send_offsets(to).wait_send()
+        send_totals(to, s).wait_send()
         send_block(to).wait_send()
         for kk in range(1, shares):
             forward_block(to, kk).wait_send()
@@ -419,7 +445,7 @@
         sides(d, sent_z)
 
 
-def gather_and_project(tokens, weight, offsets, new_rows, norm_gain, gate_weight, key_columns, scale):
+def gather_and_project(tokens, weight, offsets, new_rows, norm_gain, gate_weight, forget_bias, key_columns, scale):
     group, sub, model_width = tokens.shape
     width = line_width(group)
     depth = group // width
@@ -438,12 +464,13 @@
         out_shape=(
             jax.ShapeDtypeStruct((rows, key_columns), jnp.bfloat16),
             jax.ShapeDtypeStruct((rows, total - key_columns), jnp.bfloat16),
-            jax.ShapeDtypeStruct((rows, lanes), jnp.float32),
+            jax.ShapeDtypeStruct((offsets.shape[1], rows), jnp.float32),
             jax.ShapeDtypeStruct(offsets.shape, jnp.float32),
             jax.ShapeDtypeStruct((new_rows.shape[0], total + lanes), jnp.float32),
+            jax.ShapeDtypeStruct((group, forget_bias.shape[0], 128), jnp.float32),
         ),
-        in_specs=[hbm, hbm, hbm, vmem, vmem, vmem],
-        out_specs=(vmem, vmem, vmem, vmem, vmem),
+        in_specs=[hbm, hbm, hbm, vmem, vmem, vmem, vmem],
+        out_specs=(vmem, vmem, vmem, vmem, vmem, vmem),
         scratch_shapes=[
             pltpu.VMEM((group, groups, share, total), jnp.bfloat16),
             pltpu.VMEM((group, sub, model_width), jnp.bfloat16),
@@ -461,11 +488,13 @@
             dma((group, shares)),
             dma((group,)),
             dma((group,)),
+            dma((group,)),
+            dma((group,)),
         ],
         compiler_params=pltpu.CompilerParams(
             collective_id=0, has_side_effects=True, vmem_limit_bytes=48 * 1024 * 1024
         ),
-    )(tokens, weight.reshape(groups, share, total), offsets, new_rows, norm_gain, gate_weight)
+    )(tokens, weight.reshape(groups, share, total), offsets, new_rows, norm_gain, gate_weight, forget_bias)
 
 
 def per_device(
@@ -502,24 +531,24 @@
     )
     gate_weight = jnp.pad(gate_weight, ((0, 0), (0, -2 * heads % 128)))
     key_columns = key_weight.shape[1]
-    keys, values, gates, offsets, fresh = gather_and_project(
+    keys, values, gates, offsets, fresh, totals = gather_and_project(
         tokens.reshape(group, sub, model_width),
         weight,
         offsets,
         jnp.pad(new_rows, ((0, -seq_count % 16), (0, 0))),
         norm_gain[None],
         gate_weight,
+        forget_bias[:, None],
         key_columns,
         key_size**-0.5,
     )
-    gates = gates[:, : 2 * heads].T
     offsets = jnp.transpose(offsets, (1, 0, 2)).reshape(2 * heads, rows)
     fresh = lax.dynamic_slice_in_dim(fresh, prompt, 1, 0)
     total = weight.shape[1]
     key_new = fresh[:, :key_columns].astype(jnp.bfloat16)
     value_new = fresh[:, key_columns:total].astype(jnp.bfloat16)
     gate_new = fresh[:, total : total + heads].reshape(heads, 1)
-    log_weight = log_weights(gates, offsets, forget_bias, heads, group, pieces)
+    log_weight = log_weights(gates, offsets, forget_bias, totals, heads, group, pieces)
     query = lax.dynamic_slice_in_dim(new_query, prompt, 1, 0)
     peak, numerator, denominator = read_part(query, keys, values, log_weight, heads)
     own_score = jnp.sum(

time: 138 us -> 114 us (0.83)
  local copies, waits for them, and re-layouts: 17.7 us -> 10.1 us
  Pallas kernels: 105 us -> 97.6 us
  other arithmetic: 9.71 us -> 3.83 us
  matrix products: 3.91 us -> 1.13 us
    pallas_call x2 -> x1, Pallas kernels: 13.7 us -> 6.87 us  [gather_small(): pl.pallas_call(functools.partial(exchange_kernel, group), name=name, out_...]
    unnamed x33 -> x20, local copies, waits for them, and re-layouts: 9.23 us -> 4.49 us
    reduce_sum x1 -> x0, other arithmetic: 2.3 us -> none  [log_weights(): totals = jnp.sum(by_block, axis=2)]
    reduce_max x1, other arithmetic: 2.24 us -> 0.13 us  [read_part(): peak = jnp.max(log_weight, axis=1, keepdims=True)]
    slice x3 -> x0, local copies, waits for them, and re-layouts: 2 us -> none  [the longest x2 1 us: log_weights(): input_gate = gates[:heads] + offsets[:heads]]
    dot_general x1, matrix products: 2.03 us -> 0.25 us  [log_weights(): jnp.dot(by_block.reshape(heads * blocks, sub), later, precision=HIGHEST)]
where the time goes in v4:
time: 114 us
  Pallas kernels  97.6 us (86%)
  local copies, waits for them, and re-layouts  10.1 us (9%)
  other arithmetic  3.83 us (3%)
    pallas_call x1, Pallas kernels, gather_and_project(): pl.pallas_call(functools.partial(move_and_project, sizes), name='move_and...  90.7 us
    pallas_call x1, Pallas kernels, gather_small(): pl.pallas_call(functools.partial(exchange_kernel, group), name=name, out_...  6.87 us
    unnamed x20, local copies, waits for them, and re-layouts  4.49 us

profile of v4, /device:TPU:0, one launch (start us, length us, event | category | flops | bytes accessed | tf_op | source)
XLA Modules:
  0.0 113.6 jit_solution(16024177345022492386)
XLA Ops:
  0.6 0.0 copy-start
  0.6 0.0 copy-start.1
  0.7 0.8 fusion.31
  1.5 0.7 copy.43.forget_bias
  2.2 0.7 broadcast_in_dim.60.norm_gain
  2.9 0.8 constant_dynamic-slice_fusion.1
  3.7 0.7 pad.12.new_rows
  4.4 0.9 copy.40
  5.4 0.3 copy.42
  5.7 0.1 pad.13.gate_weight
  5.8 0.0 copy-done
  5.8 0.0 copy-done.1
  5.8 0.1 pad_maximum_fusion
  5.9 0.0 copy-start.3
  5.9 0.0 copy-start.4
  5.9 90.7 %move_and_project.1 = (bf16[1024,512]{1,0:T(8,128)(2,1)S(1)}, bf16[1024,1024]{1,0:T(8,128)(2,1)S(1)}, f32[16,1024]{1,0:T(8,128)S(1)}, f32[8,16,128]{2,1,0:T(8,12...) custom-call(bf16[8,128,2048]{2,1,0:T(8,128)(2,1)} %bitcast.110, bf16[2,128,1536]{2,1,0:T(8,128)(2,1)S(1)} %bitcast.105, ...), custom_call_target="tpu_custom_call" | custom-call | tf_op jit(solution)/shard_map/move_and_project/pallas_call | solution.py:461
  96.6 0.1 dynamic-slice_bitcast_fusion
  96.7 0.1 dynamic-slice_reduce_fusion
  96.8 0.1 copy.48
  96.9 0.1 rev.7
  96.9 0.2 reduce_window_sum.11
  97.1 0.1 rev.8
  97.2 0.0 copy-done.3
  97.2 0.1 reshape.148
  97.3 0.1 reduce_sum.69
  97.4 0.1 copy.47
  97.5 0.0 copy-done.4
  97.5 0.1 fusion.7
  97.6 0.3 fusion.1
  97.9 0.1 fusion.35
  98.0 0.0 copy-start.2
  98.0 0.1 copy.45
  98.1 0.5 fusion.37
  98.6 0.4 fusion.2
  99.0 0.1 copy.46
  99.1 0.1 select_maximum_fusion
  99.1 0.6 pad_maximum_fusion.2.mine
  99.8 6.9 %gather_read.1 = f32[8,8,384]{2,1,0:T(8,128)} custom-call(f32[8,384]{1,0:T(8,128)} %pad_maximum_fusion.2.mine), custom_call_target="tpu_custom_call" | custom-call | tf_op jit(solution)/shard_map/gather_read/pallas_call | solution.py:56
  106.6 0.7 slice_bitcast_fusion.2
  107.4 0.9 fusion.36
  108.2 0.1 copy.55
  108.3 0.1 copy.54
  108.4 0.9 slice_reduce_fusion
  109.4 0.1 copy.53
  109.5 0.8 fusion.8
  110.3 0.1 copy.56
  110.5 0.1 broadcast_bitcast_fusion
  110.6 0.1 broadcast_bitcast_fusion.1
  110.6 0.6 fusion.17
  111.3 1.0 copy.83
  112.2 0.0 copy-done.2
  112.2 1.3 %copy.84 = bf16[1,1024,1024]{2,1,0:T(8,128)(2,1)} copy(bf16[1,1024,1024]{2,1,0:T(8,128)(2,1)S(1)} %bitcast.103) | data formatting | bytes 4194304
  (15 shorter events, 0.2 us)
Async XLA Ops:
  0.6 5.1 %copy-start = (bf16[256,1024]{1,0:T(8,128)(2,1)S(1)}, bf16[256,1024]{1,0:T(8,128)(2,1)}, u32[]{:S(2)}) copy-start(bf16[256,1024]{1,0:T(8,128)(2,1)} %param.15) | copy-start | bytes 1572868
  0.6 5.1 %copy-start.1 = (bf16[256,512]{1,0:T(8,128)(2,1)S(1)}, bf16[256,512]{1,0:T(8,128)(2,1)}, u32[]{:S(2)}) copy-start(bf16[256,512]{1,0:T(8,128)(2,1)} %param.14) | copy-start | bytes 786436
  5.9 91.3 %copy-start.3 = (bf16[4,512]{1,0:T(4,128)(2,1)S(1)}, bf16[4,512]{1,0:T(4,128)(2,1)}, u32[]{:S(2)}) copy-start(bf16[4,512]{1,0:T(4,128)(2,1)} %param.12) | copy-start | bytes 12292
  5.9 91.7 %copy-start.4 = (f32[8]{0:T(128)S(1)}, f32[8]{0:T(128)}, u32[]{:S(2)}) copy-start(f32[8]{0:T(128)} %param.18) | copy-start | bytes 100
  98.0 14.2 %copy-start.2 = (f32[8,1024]{1,0:T(8,128)}, f32[8,1024]{1,0:T(8,128)S(1)}, u32[]{:S(2)}) copy-start(f32[8,1024]{1,0:T(8,128)S(1)} %get-tuple-element.21) | copy-start | bytes 98308
